TPU v7x, 128 devices: a whole 4x4x4 slice. The times are simulated.
128 devices in a mesh: ep: 16 (over z, x), tp: 8 (over y, core).
Axes of the slice: x: 4, y: 4, z: 4, core: 2. Of those that a mesh axis runs over, the one named last changes fastest.
Arguments:
- query_latent: bfloat16 [16384, 768], P(('ep', 'tp')), may hold values from -6 to 6
- kv_latent: bfloat16 [16384, 512], P(('ep', 'tp')), may hold values from -6 to 6
- rope_key: bfloat16 [16384, 64], P(('ep', 'tp')), may hold values from -6 to 6
- query_gain: float32 [768], replicated, may hold values from 0.1 to 12
- kv_gain: float32 [512], replicated, may hold values from 0.1 to 12
- query_nope_w: bfloat16 [768, 1024], P(None, 'tp'), may hold values from -0.21875 to 0.21875
- query_rope_w: bfloat16 [768, 512], P(None, 'tp'), may hold values from -0.21875 to 0.21875
- key_up_w: bfloat16 [512, 1024], P(None, 'tp'), may hold values from -0.25 to 0.25
- value_up_w: bfloat16 [512, 1024], P(None, 'tp'), may hold values from -0.25 to 0.25
- output_w: bfloat16 [1024, 2048], P('tp'), may hold values from -0.1875 to 0.1875
- expert_in: bfloat16 [16384, 2048], P(('ep', 'tp')), may hold values from -6 to 6
- moe_gain: float32 [2048], replicated, may hold values from 0.1 to 12
- routes: int32 [16384, 2], P(('ep', 'tp')), may hold values from 0 to 31, all different within a row; in each aligned block of 128 rows (0 to 127, 128 to 255, ...) at most 10 rows name the same one
- route_weight: float32 [16384, 2], P(('ep', 'tp')), may hold values from 0.1 to 1
- gate_w: bfloat16 [32, 2048, 2048], P('ep', None, 'tp'), may hold values from -0.125 to 0.125
- up_w: bfloat16 [32, 2048, 2048], P('ep', None, 'tp'), may hold values from -0.125 to 0.125
- down_w: bfloat16 [32, 2048, 2048], P('ep', 'tp'), may hold values from -0.125 to 0.125
Outputs:
- mixer_out: bfloat16 [16384, 2048], P(('ep', 'tp'))
- expert_out: bfloat16 [16384, 2048], P(('ep', 'tp'))
Inputs may be any that keep to these rules, and one draw needn't show every extreme that they name: `routes`: each row names 2 different experts; in the rows of one device no expert is named more than 10 times.
All inputs are finite; a program needn't handle non-finite values.
Results may differ from a plain program's by a relative error of at most 0.015.
The roundings to bfloat16 on the way count: a program that leaves them out, or rounds other values in their place, can miss the bound.
Values may be sent and summed in bfloat16 or wider, within the bound.
No kernel may reach another device: no remote copies, remote signals or barrier semaphores. Data moves between devices by JAX's collectives and lax.ppermute only.
A program may use at most 128 MiB of HBM per device.

v0:
```python
import functools
import math

import jax
import jax.numpy as jnp
import numpy as np
from jax import lax
from jax.experimental import pallas as pl
from jax.experimental.pallas import tpu as pltpu
from jax.sharding import PartitionSpec as P


NOPE = 128
ROPE = 64
VDIM = 128
THETA = 10000.0
CHUNK = 24
HALF = 12
CAP = 10
BF = jnp.bfloat16
F32 = jnp.float32
LOG2E = 1.4426950408889634


def dot(a, b, dims=(((1,), (0,)), ((), ()))):
    return lax.dot_general(a, b, dims, preferred_element_type=F32)


def pairs(move):
    result = []
    for device in range(128):
        ep, tp = divmod(device, 8)
        z, x, y, core = ep // 4, ep % 4, tp // 2, tp % 2
        dz, dx, dy, dc = move(core)
        ep = ((z + dz) % 4) * 4 + (x + dx) % 4
        tp = ((y + dy) % 4) * 2 + (core ^ dc)
        result.append((device, ep * 8 + tp))
    return result


def send(a, move):
    return lax.ppermute(a, ("ep", "tp"), pairs(move))


def swap(a):
    return send(a, lambda core: (0, 0, 0, 1))


def along_y(d):
    return lambda core: (0, 0, -d if core else d, 0)


def plain_y(d):
    return lambda core: (0, 0, d, 0)


def along_one(d):
    return lambda core: (0, d, 0, 0) if core else (d, 0, 0, 0)


def along_two(d):
    return lambda core: (d, 0, 0, 0) if core else (0, d, 0, 0)


def ring(block, along):
    behind = send(block, along(1))
    ahead = send(block, along(-1))
    far = send(behind, along(1))
    return behind, ahead, far


def ring_halves(one, two, along):
    one_behind = send(one, along(1))
    two_ahead = send(two, along(-1))
    two_behind = send(two, along(1))
    one_ahead = send(one, along(-1))
    one_far = send(one_behind, along(1))
    two_far = send(two_ahead, along(-1))
    return (one_behind, two_behind), (one_ahead, two_ahead), (one_far, two_far)


def slots_of(route, rank):
    return (route >> 1) * CHUNK + (route & 1) * HALF + rank


def upright(row):
    count = row.shape[1]
    i = lax.broadcasted_iota(jnp.int32, (count, count), 0)
    j = lax.broadcasted_iota(jnp.int32, (count, count), 1)
    spread = jnp.where(i == j, row.astype(F32), 0.0)
    return jnp.sum(spread, axis=1, keepdims=True).astype(jnp.int32)


def dispatch_body(x_ref, gain_ref, row_ref, out_ref):
    floats = x_ref[...].astype(F32)
    center = floats - jnp.mean(floats, axis=-1, keepdims=True)
    variance = jnp.mean(center * center, axis=-1, keepdims=True)
    normed = (center * lax.rsqrt(variance + 1e-05) * gain_ref[...][None, :]).astype(BF)
    count = x_ref.shape[0]
    cols = [upright(row_ref[k : k + 1, :]) for k in range(2)]
    j = lax.broadcasted_iota(jnp.int32, (count, count), 0)
    i = lax.broadcasted_iota(jnp.int32, (count, count), 1)
    earlier = j < i
    total = out_ref.shape[0]
    number = lax.broadcasted_iota(jnp.int32, (total, count), 0)
    select = None
    for k in range(2):
        mine = row_ref[k : k + 1, :]
        same = (cols[0] == mine) | (cols[1] == mine)
        rank = jnp.sum(jnp.where(same & earlier, 1.0, 0.0), axis=0, keepdims=True)
        hit = number == slots_of(mine, rank.astype(jnp.int32))
        select = hit if select is None else select | hit
    pick = jnp.where(select, 1.0, 0.0).astype(BF)
    out_ref[...] = dot(pick, normed).astype(BF)


def dispatch(x, gain, routes):
    return pl.pallas_call(
        dispatch_body,
        out_shape=jax.ShapeDtypeStruct((16 * CHUNK, x.shape[1]), BF),
        name="dispatch",
    )(x, gain, routes.T)


def combine_body(back_ref, row_ref, w_ref, out_ref):
    count = row_ref.shape[1]
    i = lax.broadcasted_iota(jnp.int32, (count, count), 0)
    j = lax.broadcasted_iota(jnp.int32, (count, count), 1)
    earlier = j < i
    total = back_ref.shape[0]
    number = lax.broadcasted_iota(jnp.int32, (count, total), 1)
    weight = w_ref[...]
    weight = weight / jnp.sum(weight, axis=-1, keepdims=True)
    back = back_ref[...]
    result = None
    for k in range(2):
        mine = upright(row_ref[k : k + 1, :])
        same = (row_ref[0:1, :] == mine) | (row_ref[1:2, :] == mine)
        rank = jnp.sum(jnp.where(same & earlier, 1.0, 0.0), axis=1, keepdims=True)
        hit = number == slots_of(mine, rank.astype(jnp.int32))
        pick = jnp.where(hit, 1.0, 0.0).astype(BF)
        term = dot(pick, back) * weight[:, k : k + 1]
        result = term if result is None else result + term
    out_ref[...] = result.astype(BF)


def combine(back, routes, route_weight):
    return pl.pallas_call(
        combine_body,
        out_shape=jax.ShapeDtypeStruct((routes.shape[0], back.shape[1]), BF),
        name="combine",
    )(back, routes.T, route_weight)


def packing(flip):
    rows, cols = 16 * 2 * CAP, 16 * CHUNK
    shape = (cols, rows) if flip else (rows, cols)
    r = lax.broadcasted_iota(jnp.int32, shape, flip)
    c = lax.broadcasted_iota(jnp.int32, shape, 1 - flip)
    per = 16 * CAP
    slot = ((r % per) // CAP) * CHUNK + (r // per) * HALF + r % CAP
    return (slot == c).astype(BF)


def pack_body(pick_ref, x_ref, one_ref, two_ref):
    rows = one_ref.shape[0]
    packed = dot(pick_ref[...], x_ref[...]).astype(BF)
    one_ref[...] = packed[:rows]
    two_ref[...] = packed[rows:]


def columns(rows, width=512):
    return pl.BlockSpec((rows, width), lambda n: (0, n))


def whole(shape):
    return pl.BlockSpec(shape, lambda n: (0,) * len(shape))


def pack(pick, arrived):
    rows, width = arrived.shape
    half = pick.shape[0] // 2
    return pl.pallas_call(
        pack_body,
        grid=(2,),
        in_specs=[whole(pick.shape), columns(rows, width // 2)],
        out_specs=[columns(half, width // 2)] * 2,
        out_shape=[jax.ShapeDtypeStruct((half, width), BF)] * 2,
        name="pack",
    )(pick, arrived)


def unpack_body(pick_ref, *refs):
    out_ref = refs[-1]
    halves = []
    for k in range(2):
        a, b, c = refs[k:6:2]
        halves.append((a[...].astype(F32) + b[...].astype(F32) + c[...].astype(F32)).astype(BF))
    summed = jnp.concatenate(halves, axis=0)
    out_ref[...] = dot(pick_ref[...], summed).astype(BF)


def unpack(pick, *terms):
    rows, width = terms[0][0].shape
    return pl.pallas_call(
        unpack_body,
        grid=(2,),
        in_specs=[whole(pick.shape)] + [columns(rows, width // 2)] * 6,
        out_specs=columns(pick.shape[0], width // 2),
        out_shape=jax.ShapeDtypeStruct((pick.shape[0], width), BF),
        name="unpack",
    )(pick, *[a for pair in terms for a in pair])


def add_body(*refs):
    count = len(refs) // 3
    for k in range(count):
        a, b = refs[2 * k], refs[2 * k + 1]
        refs[2 * count + k][...] = (a[...].astype(F32) + b[...].astype(F32)).astype(BF)


def add(*pairs):
    rows, width = pairs[0][0].shape
    count = len(pairs)
    block = pl.BlockSpec((rows // 2, width), lambda n: (n, 0))
    return pl.pallas_call(
        add_body,
        grid=(2,),
        in_specs=[block] * 2 * count,
        out_specs=[block] * count,
        out_shape=[jax.ShapeDtypeStruct((rows, width), BF)] * count,
        name="add",
    )(*[a for pair in pairs for a in pair])


def ffn_body(count, *refs):
    xs = refs[: 2 * count]
    sources = refs[2 * count : 2 * count + 6]
    outs = refs[2 * count + 6 : 4 * count + 6]
    gates, uppers, downs, sems = refs[4 * count + 6 :]
    copies = []
    for expert in range(2):
        for half in range(2):
            for k, target in enumerate((gates, uppers, downs)):
                number = len(copies)
                copies.append(
                    pltpu.make_async_copy(
                        sources[half * 3 + k].at[expert],
                        target.at[expert * 2 + half],
                        sems.at[number],
                    )
                )
    for copy in copies:
        copy.start()
    rows = xs[0].shape[0]
    for expert in range(2):
        mine = xs[expert::2]
        x = mine[0][...] if count == 1 else jnp.concatenate([r[...] for r in mine], axis=0)
        hidden = []
        for half in range(2):
            at = expert * 2 + half
            for k in range(3):
                copies[at * 3 + k].wait()
            gate = jnp.minimum(dot(x, gates[at]), 7.0)
            upper = jnp.clip(dot(x, uppers[at]), -7.0, 7.0)
            hidden.append((gate * jax.nn.sigmoid(1.702 * gate) * (upper + 1.0)).astype(BF))
        total = dot(hidden[0], downs[expert * 2]) + dot(hidden[1], downs[expert * 2 + 1])
        total = total.astype(BF)
        for k in range(count):
            outs[2 * k + expert][...] = total[k * rows : (k + 1) * rows]


def ffn(weights, *xs):
    rows, width = xs[0][0].shape
    count = len(xs)
    inner = weights[0].shape[2]
    vmem = pl.BlockSpec(memory_space=pltpu.VMEM)
    out = jax.ShapeDtypeStruct((rows, width), BF)
    outs = pl.pallas_call(
        functools.partial(ffn_body, count),
        in_specs=[vmem] * 2 * count + [pl.BlockSpec(memory_space=pl.ANY)] * 6,
        out_specs=[vmem] * 2 * count,
        out_shape=[out] * 2 * count,
        scratch_shapes=[
            pltpu.VMEM((4, width, inner), BF),
            pltpu.VMEM((4, width, inner), BF),
            pltpu.VMEM((4, inner, width), BF),
            pltpu.SemaphoreType.DMA((12,)),
        ],
        cost_estimate=pl.CostEstimate(
            flops=12 * rows * count * width * 512, bytes_accessed=16 << 20, transcendentals=0
        ),
        name="ffn",
    )(*[a for pair in xs for a in pair], *weights)
    return [tuple(outs[2 * k : 2 * k + 2]) for k in range(count)]


def experts_half(
    expert_in, moe_gain, routes, route_weight, gate_w, up_w, down_w
):
    width = expert_in.shape[1]
    outgoing = dispatch(expert_in, moe_gain, routes)
    weights = (gate_w, up_w, down_w, swap(gate_w), swap(up_w), swap(down_w))
    arrived = lax.all_to_all(
        outgoing.reshape(16, CHUNK, width), "ep", split_axis=0, concat_axis=0, tiled=True
    ).reshape(16 * CHUNK, width)
    own = pack(packing(0), arrived)
    below, above, far = ring_halves(*own, plain_y)
    (below0, above1), own_out = ffn(weights, (below[0], above[1]), own)
    from_above0 = send(below0, plain_y(-1))
    from_below1 = send(above1, plain_y(1))
    (far0, far1), (above0, below1) = ffn(weights, far, (above[0], below[1]))
    far0 = send(far0, plain_y(1))
    far1 = send(far1, plain_y(-1))
    above0, below1 = add((above0, far0), (below1, far1))
    from_below0 = send(above0, plain_y(1))
    from_above1 = send(below1, plain_y(-1))
    back = unpack(packing(1), own_out, (from_below0, from_below1), (from_above0, from_above1))
    back = lax.all_to_all(
        back.reshape(16, CHUNK, width), "ep", split_axis=0, concat_axis=0, tiled=True
    ).reshape(16 * CHUNK, width)
    return combine(back, routes, route_weight)


SCALE2 = LOG2E / math.sqrt(NOPE + ROPE)
QLAT = 768
KVLAT = 512
LATENT = 1536
KEYS = 512
PIECE = KEYS + KEYS // 2 + 4 * VDIM
NT = (((1,), (1,)), ((), ()))
LIMIT = 2.0**80


def prepare_body(q_ref, kv_ref, rot_ref, qg_ref, kvg_ref, out_ref):
    for ref, gain, at in ((q_ref, qg_ref, 0), (kv_ref, kvg_ref, QLAT)):
        floats = ref[...].astype(F32)
        square = jnp.mean(floats * floats, axis=-1, keepdims=True)
        normed = floats * lax.rsqrt(square + 1e-06) * gain[...][None, :]
        out_ref[:, at : at + ref.shape[1]] = normed.astype(BF)
    rot = rot_ref[...]
    both = jnp.concatenate([rot, jnp.zeros_like(rot)], axis=1)
    out_ref[:, QLAT + KVLAT : QLAT + KVLAT + 128] = both
    out_ref[:, QLAT + KVLAT + 128 :] = jnp.zeros((rot.shape[0], 128), BF)


def prepare(query_latent, kv_latent, key_rot, query_gain, kv_gain):
    return pl.pallas_call(
        prepare_body,
        out_shape=jax.ShapeDtypeStruct((query_latent.shape[0], LATENT), BF),
        name="prepare",
    )(query_latent, kv_latent, key_rot, query_gain, kv_gain)


def heads_body(*refs):
    blocks = refs[:8]
    key_ref, value_ref, nope_ref, rope_ref, cos_ref, sin_ref = refs[8:14]
    kv_ref, low_ref, high_ref = refs[14:]
    kv = jnp.concatenate([r[:, QLAT : QLAT + KVLAT] for r in blocks], axis=0)
    keys = dot(kv, key_ref[...]).astype(BF)
    values = dot(value_ref[...].T, kv, NT).astype(BF)
    rots = jnp.concatenate(
        [r[:, QLAT + KVLAT : QLAT + KVLAT + 128] for r in blocks], axis=0
    ).astype(F32)
    half = KEYS // 2
    for k in range(2):
        at = k * KEYS
        to = k * PIECE
        pair = rots[at : at + half] + pltpu.roll(rots[at + half : at + KEYS], ROPE, 1)
        kv_ref[to : to + KEYS, :] = keys[at : at + KEYS]
        kv_ref[to + KEYS : to + KEYS + half, :] = pair.astype(BF)
        for c in range(4):
            row = to + KEYS + half + 128 * c
            kv_ref[row : row + 128, :] = values[:, at + 128 * c : at + 128 * (c + 1)]
    query_in = jnp.concatenate([r[:, :QLAT] for r in blocks], axis=0)
    query = dot(jnp.concatenate([nope_ref[...].T, rope_ref[...]], axis=0), query_in, NT)
    first = query[NOPE : NOPE + ROPE // 2]
    second = query[NOPE + ROPE // 2 :]
    cosine = cos_ref[...]
    sine = sin_ref[...]
    rot = jnp.concatenate([first * cosine - second * sine, second * cosine + first * sine], axis=0)
    nope = query[:NOPE].astype(BF)
    rot = rot.astype(BF)
    blank = jnp.zeros_like(rot)
    low_ref[...] = jnp.concatenate([nope, rot, blank], axis=0)
    high_ref[...] = jnp.concatenate([nope, blank, rot], axis=0)


def heads(blocks, key_w, value_w, nope_w, rope_w, cosine, sine):
    rows = 8 * blocks[0].shape[0]
    query = jax.ShapeDtypeStruct((256, rows), BF)
    return pl.pallas_call(
        heads_body,
        out_shape=[jax.ShapeDtypeStruct((2 * PIECE, 128), BF), query, query],
        cost_estimate=pl.CostEstimate(
            flops=2 * rows * (QLAT * 192 + KVLAT * 256), bytes_accessed=6 << 20, transcendentals=0
        ),
        name="heads",
    )(*blocks, key_w, value_w, nope_w, rope_w.T, cosine, sine)


def join_body(a_ref, b_ref, c_ref, d_ref, one_ref, two_ref):
    rows = a_ref.shape[0]
    one_ref[:rows, :] = a_ref[...]
    one_ref[rows:, :] = b_ref[...]
    two_ref[:rows, :] = c_ref[...]
    two_ref[rows:, :] = d_ref[...]


def join(blocks):
    rows = blocks[0].shape[0]
    out = jax.ShapeDtypeStruct((2 * rows, 128), BF)
    return pl.pallas_call(join_body, out_shape=[out] * 2, name="join")(*blocks)


def load_piece(ref, k):
    at = pl.multiple_of(k * PIECE, PIECE)
    half = KEYS // 2
    pair = ref[pl.ds(at + KEYS, half), :]
    left = jnp.concatenate([ref[pl.ds(at, half), :], pair], axis=1)
    right = jnp.concatenate([ref[pl.ds(at + half, half), :], pair], axis=1)
    value = [ref[pl.ds(at + KEYS + half + 128 * c, 128), :] for c in range(4)]
    return left, right, jnp.concatenate(value, axis=1)


def own_body(kpos_ref, qpos_ref, low_ref, high_ref, kv_ref, *refs):
    m_ref, l_ref, acc_ref = refs[-3:]
    tile = 256
    half = KEYS // 2
    pieces = [load_piece(kv_ref, k) for k in range(2)]
    lefts = [pieces[0][0], pieces[0][1], pieces[1][0], pieces[1][1]]
    value = jnp.concatenate([pieces[0][2], pieces[1][2]], axis=1)
    for part in range(low_ref.shape[1] // tile):
        cols = slice(part * tile, (part + 1) * tile)
        scores = []
        for k, left in enumerate(lefts):
            s = dot(left, (high_ref if k % 2 else low_ref)[:, cols])
            allowed = kpos_ref[k * half : (k + 1) * half, :] <= qpos_ref[:, cols]
            scores.append(jnp.where(allowed, s, -1e30))
        peaks = [jnp.max(s, axis=0, keepdims=True) for s in scores]
        m = jnp.maximum(jnp.maximum(peaks[0], peaks[1]), jnp.maximum(peaks[2], peaks[3]))
        base = m * SCALE2
        probs = [jnp.exp2(s * SCALE2 - base) for s in scores]
        sums = [jnp.sum(p, axis=0, keepdims=True) for p in probs]
        m_ref[:, cols] = m
        l_ref[:, cols] = (sums[0] + sums[1]) + (sums[2] + sums[3])
        acc_ref[:, cols] = dot(value, jnp.concatenate([p.astype(BF) for p in probs], axis=0))


def own_attention(low, high, kv, positions):
    rows = low.shape[1]
    thin = jax.ShapeDtypeStruct((1, rows), F32)
    vmem = pl.BlockSpec(memory_space=pltpu.VMEM)
    return pl.pallas_call(
        own_body,
        in_specs=[vmem] * 5,
        out_specs=[vmem] * 3,
        out_shape=[thin, thin, jax.ShapeDtypeStruct((VDIM, rows), F32)],
        cost_estimate=pl.CostEstimate(
            flops=2 * rows * rows * 384, bytes_accessed=4 << 20, transcendentals=rows * rows
        ),
        name="own_attention",
    )(positions.reshape(-1, 1), positions.reshape(1, -1), low, high, kv)


def more_body(arrays, first, final, flags_ref, low_ref, high_ref, *refs):
    pieces = refs[:arrays]
    m_in, l_in, acc_in = refs[arrays : arrays + 3]
    keys_ref, sems = refs[-2:]
    m_ref, l_ref, acc_ref = refs[-5:-2]
    size = pieces[0].shape[0]

    def fetch(ref, number):
        target = keys_ref.at[pl.ds(pl.multiple_of(number * size, size), size)]
        return pltpu.make_async_copy(ref, target, sems.at[number])

    for number, ref in enumerate(pieces):
        fetch(ref, number).start()
    tile = 256
    tiles = low_ref.shape[1] // tile

    def start():
        m_ref[...] = m_in[...]
        l_ref[...] = l_in[...]
        acc_ref[...] = acc_in[...]

    def score(piece, t):
        cols = slice(t * tile, (t + 1) * tile)
        return dot(piece[0], low_ref[:, cols]), dot(piece[1], high_ref[:, cols])

    def over(step, wait):
        def array(number, _):
            if wait:
                fetch(pieces[0], number).wait()

            def one(k, _):
                @pl.when(flags_ref[first + 2 * number + k] != 0)
                def _():
                    step(2 * number + k)

                return 0

            lax.fori_loop(0, 2, one, 0)
            return 0

        lax.fori_loop(0, arrays, array, 0)

    def weigh(s, t):
        cols = slice(t * tile, (t + 1) * tile)
        base = m_ref[:, cols] * SCALE2
        p = jnp.exp2(s[0] * SCALE2 - base)
        q = jnp.exp2(s[1] * SCALE2 - base)
        l_ref[:, cols] += jnp.sum(p, axis=0, keepdims=True) + jnp.sum(q, axis=0, keepdims=True)
        return jnp.concatenate([p.astype(BF), q.astype(BF)], axis=0)

    def gather(piece, probs, t):
        cols = slice(t * tile, (t + 1) * tile)
        acc_ref[:, cols] += dot(piece[2], probs)

    def quick(k):
        block = [load_piece(keys_ref, 2 * k), load_piece(keys_ref, 2 * k + 1)]
        steps = [(piece, t) for piece in block for t in range(tiles)]
        s = score(*steps[0])
        before = None
        for i, (_, t) in enumerate(steps):
            after = score(*steps[i + 1]) if i + 1 < len(steps) else None
            if before is not None:
                gather(steps[i - 1][0], before, steps[i - 1][1])
            before = weigh(s, t)
            s = after
        gather(steps[-1][0], before, steps[-1][1])

    def careful(k):
        def one(i, _):
            piece = load_piece(keys_ref, 2 * k + i // tiles)
            cols = pl.ds(pl.multiple_of((i % tiles) * tile, tile), tile)
            p = dot(piece[0], low_ref[:, cols])
            q = dot(piece[1], high_ref[:, cols])
            before = m_ref[:, cols]
            peak = jnp.maximum(jnp.max(p, axis=0, keepdims=True), jnp.max(q, axis=0, keepdims=True))
            m = jnp.maximum(before, peak)
            alpha = jnp.exp2((before - m) * SCALE2)
            p = jnp.exp2(p * SCALE2 - m * SCALE2)
            q = jnp.exp2(q * SCALE2 - m * SCALE2)
            m_ref[:, cols] = m
            total = jnp.sum(p, axis=0, keepdims=True) + jnp.sum(q, axis=0, keepdims=True)
            l_ref[:, cols] = l_ref[:, cols] * alpha + total
            probs = jnp.concatenate([p.astype(BF), q.astype(BF)], axis=0)
            acc_ref[:, cols] = acc_ref[:, cols] * alpha + dot(piece[2], probs)
            return 0

        lax.fori_loop(0, 2 * tiles, one, 0)

    start()
    over(quick, True)
    safe = jnp.where(l_ref[...] < LIMIT, 0.0, 1.0)

    @pl.when(jnp.max(safe) > 0.0)
    def _():
        start()
        over(careful, False)

    if final:
        done = (acc_ref[...] / l_ref[...]).astype(BF)
        for b in range(4):
            refs[arrays + 3 + b][...] = done[:, 256 * b : 256 * (b + 1)]


def more_attention(low, high, arrays, flags, first, state, final=False):
    rows = low.shape[1]
    keys = 4 * len(arrays) * KEYS
    shapes = [(1, rows), (1, rows), (VDIM, rows)]
    if final:
        out_shape = [jax.ShapeDtypeStruct((VDIM, rows // 4), BF)] * 4
        scratch = [pltpu.VMEM(s, F32) for s in shapes]
    else:
        out_shape = [jax.ShapeDtypeStruct(s, F32) for s in shapes]
        scratch = []
    vmem = pl.BlockSpec(memory_space=pltpu.VMEM)
    count = len(arrays)
    scratch += [
        pltpu.VMEM((count * arrays[0].shape[0], 128), BF),
        pltpu.SemaphoreType.DMA((count,)),
    ]
    return pl.pallas_call(
        functools.partial(more_body, count, first, final),
        in_specs=[pl.BlockSpec(memory_space=pltpu.SMEM), vmem, vmem]
        + [pl.BlockSpec(memory_space=pl.ANY)] * count
        + [vmem] * 3,
        out_specs=[vmem] * len(out_shape),
        out_shape=out_shape,
        scratch_shapes=scratch,
        cost_estimate=pl.CostEstimate(
            flops=rows * keys * 384, bytes_accessed=4 << 20, transcendentals=rows * keys
        ),
        name="more_attention",
    )(flags, low, high, *arrays, *state)


def project_body(*refs):
    left = jnp.concatenate([r[...] for r in refs[:4]], axis=0)
    right = jnp.concatenate([r[...] for r in refs[4:8]], axis=0)
    mine, other = refs[8:]
    result = dot(left, right, (((0,), (0,)), ((), ())))
    rows = mine.shape[0]
    mine[...] = result[:rows]
    other[...] = result[rows:].astype(BF)


def project(attended, blocks):
    rows = attended[0].shape[1] // 2
    width = blocks[0].shape[1]
    return pl.pallas_call(
        project_body,
        grid=(width // 512,),
        in_specs=[whole(a.shape) for a in attended] + [columns(128)] * 4,
        out_specs=[columns(rows)] * 2,
        out_shape=[
            jax.ShapeDtypeStruct((rows, width), F32),
            jax.ShapeDtypeStruct((rows, width), BF),
        ],
        name="project",
    )(*attended, *blocks)


def angles(positions):
    half = ROPE // 2
    freq = 1.0 / THETA ** (jnp.arange(half, dtype=F32) * 2.0 / ROPE)
    return positions.astype(F32), freq


def turn(values):
    half = ROPE // 2
    return jnp.concatenate([-values[:, half:], values[:, :half]], axis=-1)


LINE = (0, 1, -1, 2)


def sources():
    near = [(d, 0) for d in LINE]
    wide = [(a, b) for b in (1, -1) for a in LINE]
    far = [(a, 2) for a in LINE]
    return near + wide + far


def own_block(query_latent, kv_latent, rope_key, query_gain, kv_gain):
    local = query_latent.shape[0]
    first = (lax.axis_index("ep") * 8 + lax.axis_index("tp")) * local
    place, freq = angles(first + jnp.arange(local, dtype=jnp.int32))
    angle = place[:, None] * freq[None, :]
    angle = jnp.concatenate([angle, angle], axis=-1)
    key_in = rope_key.astype(F32)
    key_rot = (key_in * jnp.cos(angle) + turn(key_in) * jnp.sin(angle)).astype(BF)
    return prepare(query_latent, kv_latent, key_rot, query_gain, kv_gain)


def mixer(query_latent, query_nope_w, query_rope_w, key_up_w, value_up_w, output_w, block):
    local = query_latent.shape[0]
    group = local * 8
    ep = lax.axis_index("ep")
    tp = lax.axis_index("tp")
    z, x = ep // 4, ep % 4
    y, core = tp // 2, tp % 2
    behind, ahead, far = ring(block, along_y)
    outputs = (output_w, *ring(output_w, along_y))
    blocks = [block, swap(block), behind, swap(ahead), ahead, swap(behind), far, swap(far)]
    turned = 1 - 2 * core
    chips = (y + turned * np.array([0, -1, 1, 2], np.int32)) % 4
    one = np.array([s[0] for s in sources()], np.int32)
    two = np.array([s[1] for s in sources()], np.int32)
    dz = jnp.where(core == 0, one, two)
    dx = jnp.where(core == 0, two, one)
    flags = (((z - dz) % 4) * 4 + (x - dx) % 4 < ep).astype(jnp.int32)
    order = chips[:, None] * 2 + (core ^ np.array([[0, 1]], np.int32))
    inside = (order.reshape(8, 1) * local + np.arange(local, dtype=np.int32)[None, :]).reshape(-1)
    place, freq = angles(ep * group + inside)
    angle = freq[:, None] * place[None, :]
    turns = jnp.cos(angle), jnp.sin(angle)
    kv, low, high = heads(blocks, key_up_w, value_up_w, query_nope_w, query_rope_w, *turns)
    one, two = join([kv, *ring(kv, along_one)])
    behind, ahead, far = ring_halves(one, two, along_two)
    state = own_attention(low, high, kv, inside)
    state = more_attention(low, high, (one, two), flags, 0, state)
    state = more_attention(low, high, (*behind, *ahead), flags, 4, state)
    attended = more_attention(low, high, far, flags, 12, state, final=True)
    attended = (
        attended[0],
        send(attended[2], along_y(1)),
        send(attended[1], along_y(-1)),
        send(attended[3], along_y(2)),
    )
    mine, other = project(attended, outputs)
    return add((mine, swap(other)))[0]


def per_device(
    query_latent,
    kv_latent,
    rope_key,
    query_gain,
    kv_gain,
    query_nope_w,
    query_rope_w,
    key_up_w,
    value_up_w,
    output_w,
    expert_in,
    moe_gain,
    routes,
    route_weight,
    gate_w,
    up_w,
    down_w,
):
    block = own_block(query_latent, kv_latent, rope_key, query_gain, kv_gain)
    mixer_out = mixer(
        query_latent, query_nope_w, query_rope_w, key_up_w, value_up_w, output_w, block
    )
    expert_out = experts_half(
        expert_in, moe_gain, routes, route_weight, gate_w, up_w, down_w
    )
    return (mixer_out, expert_out)


def solution(mesh):
    placed = (
        P(("ep", "tp"), None),
        P(("ep", "tp"), None),
        P(("ep", "tp"), None),
        P(),
        P(),
        P(None, "tp"),
        P(None, "tp"),
        P(None, "tp"),
        P(None, "tp"),
        P("tp", None),
        P(("ep", "tp"), None),
        P(),
        P(("ep", "tp"), None),
        P(("ep", "tp"), None),
        P("ep", None, "tp"),
        P("ep", None, "tp"),
        P("ep", "tp", None),
    )
    return jax.shard_map(
        per_device,
        mesh=mesh,
        in_specs=placed,
        out_specs=(P(("ep", "tp"), None), P(("ep", "tp"), None)),
        check_vma=False,
    )
```

profile of v0, /device:TPU:103, one launch (start us, length us, event | category | flops | bytes accessed | tf_op | source)
XLA Modules:
  0.0 287.6 jit_solution(4762879498405036467)
XLA Ops:
  8.4 3.1 %dispatch.1 = bf16[384,2048]{1,0:T(8,128)(2,1)} custom-call(bf16[128,2048]{1,0:T(8,128)(2,1)} %x_ref.1, f32[2048]{0:T(1024)} %gain_ref.1, s32[2,128]{1,0:T(2,128)} %bitcast.18), custom_call_target="tpu_custom_call" | custom-call | tf_op jit(solution)/shard_map/dispatch/pallas_call | solution.py:118
  11.6 6.5 %all-to-all-start = ((bf16[16,24,2048]{2,1,0:T(8,128)(2,1)}), bf16[16,24,2048]{2,1,0:T(8,128)(2,1)}, u32[]{:S(2)}, u32[]{:S(2)}) async-start(bf16[16,24,2048]{2,1,0:T(8,128)(2,1)} %bitcast.12), calls=%async_computation | async-start | bytes 3145728 | tf_op jit(solution)/shard_map/all_to_all | solution.py:304
  21.7 4.2 %collective-permute-done.5.refs_6_ = bf16[128,1536]{1,0:T(8,128)(2,1)} collective-permute-done((bf16[128,1536]{1,0:T(8,128)(2,1)S(1)}, bf16[128,1536]{1,0:T(8,128)(2,1)}, u32[]{:S(2)}, u32[]{:S(2)}) %collective-permute-start.5) | collective-permute-done | bytes 393248 | tf_op jit(solution)/shard_map/ppermute | solution.py:42
  31.3 4.4 %heads.1 = (bf16[2560,128]{1,0:T(8,128)(2,1)}, bf16[256,1024]{1,0:T(8,128)(2,1)}, bf16[256,1024]{1,0:T(8,128)(2,1)}) custom-call(bf16[128,1536]{1,0:T(8,128)(2,1)} %prepare.1.refs_0_, bf16[128,1536]{1,0:T(8,128)(2,1)} %copy-done.23, bf16[128,1536]{1,0:T(8,128)(2,1)} %copy-done.21, bf16[128,1536]{1,0:T(8,128)(2,1)} %copy-done.24, ...), custom_call_target="tpu_custom_call" | custom-call | flops 570425344 | bytes 6291456 | tf_op jit(solution)/shard_map/heads/pallas_call | solution.py:392
  42.1 4.6 %collective-permute-done.7.b_ref = bf16[2560,128]{1,0:T(8,128)(2,1)S(1)} collective-permute-done((bf16[2560,128]{1,0:T(8,128)(2,1)}, bf16[2560,128]{1,0:T(8,128)(2,1)S(1)}, u32[]{:S(2)}, u32[]{:S(2)}) %collective-permute-start.7) | collective-permute-done | bytes 655392 | tf_op jit(solution)/shard_map/ppermute | solution.py:42
  48.9 9.6 %collective-permute-done.23.refs_0_ = bf16[160,2048]{1,0:T(8,128)(2,1)S(1)} collective-permute-done((bf16[160,2048]{1,0:T(8,128)(2,1)}, bf16[160,2048]{1,0:T(8,128)(2,1)S(1)}, u32[]{:S(2)}, u32[]{:S(2)}) %collective-permute-start.23) | collective-permute-done | bytes 655392 | tf_op jit(solution)/shard_map/ppermute | solution.py:42
  58.5 4.3 %collective-permute-done.24.refs_1_ = bf16[160,2048]{1,0:T(8,128)(2,1)S(1)} collective-permute-done((bf16[160,2048]{1,0:T(8,128)(2,1)}, bf16[160,2048]{1,0:T(8,128)(2,1)S(1)}, u32[]{:S(2)}, u32[]{:S(2)}) %collective-permute-start.24) | collective-permute-done | bytes 655392 | tf_op jit(solution)/shard_map/ppermute | solution.py:42
  65.2 11.7 %collective-permute-done.30.refs_2_ = bf16[160,2048]{1,0:T(8,128)(2,1)S(1)} collective-permute-done((bf16[160,2048]{1,0:T(8,128)(2,1)}, bf16[160,2048]{1,0:T(8,128)(2,1)S(1)}, u32[]{:S(2)}, u32[]{:S(2)}) %collective-permute-start.30) | collective-permute-done | bytes 655392 | tf_op jit(solution)/shard_map/ppermute | solution.py:42
  78.4 8.2 %collective-permute-done.28.refs_0_ = bf16[160,2048]{1,0:T(8,128)(2,1)S(1)} collective-permute-done((bf16[160,2048]{1,0:T(8,128)(2,1)S(1)}, bf16[160,2048]{1,0:T(8,128)(2,1)S(1)}, u32[]{:S(2)}, u32[]{:S(2)}) %collective-permute-start.28) | collective-permute-done | bytes 655392 | tf_op jit(solution)/shard_map/ppermute | solution.py:42
  87.5 3.6 %collective-permute-done.29.refs_1_ = bf16[160,2048]{1,0:T(8,128)(2,1)} collective-permute-done((bf16[160,2048]{1,0:T(8,128)(2,1)S(1)}, bf16[160,2048]{1,0:T(8,128)(2,1)}, u32[]{:S(2)}, u32[]{:S(2)}) %collective-permute-start.29) | collective-permute-done | bytes 655392 | tf_op jit(solution)/shard_map/ppermute | solution.py:42
  91.1 10.0 %ffn.3 = (bf16[160,2048]{1,0:T(8,128)(2,1)}, bf16[160,2048]{1,0:T(8,128)(2,1)}, bf16[160,2048]{1,0:T(8,128)(2,1)}, bf16[160,2048]{1,0:T(8,128)(2,1)}) custom-call(bf16[160,2048]{1,0:T(8,128)(2,1)} %copy-done.16, bf16[160,2048]{1,0:T(8,128)(2,1)} %collective-permute-done.29.refs_1_, bf16[160,2048]{1,0:T(8,128)(2,1)} %copy-done.14, ...), custom_call_target="tpu_custom_call" | custom-call | flops 4026531840 | bytes 16777216 | tf_op jit(solution)/shard_map/ffn/pallas_call | solution.py:279
  103.0 3.3 %join.1 = (bf16[5120,128]{1,0:T(8,128)(2,1)}, bf16[5120,128]{1,0:T(8,128)(2,1)}) custom-call(bf16[2560,128]{1,0:T(8,128)(2,1)} %get-tuple-element.36.a_ref.kv_ref, bf16[2560,128]{1,0:T(8,128)(2,1)} %copy-done.3, bf16[2560,128]{1,0:T(8,128)(2,1)} %copy-done.5, bf16[2560,128]{1,0:T(8,128)(2,1)} %copy-done.7), custom_call_target="tpu_custom_call" | custom-call | tf_op jit(solution)/shard_map/join/pallas_call | solution.py:413
  110.9 10.0 %ffn.2 = (bf16[160,2048]{1,0:T(8,128)(2,1)}, bf16[160,2048]{1,0:T(8,128)(2,1)}, bf16[160,2048]{1,0:T(8,128)(2,1)}, bf16[160,2048]{1,0:T(8,128)(2,1)}) custom-call(bf16[160,2048]{1,0:T(8,128)(2,1)} %copy-done.12, bf16[160,2048]{1,0:T(8,128)(2,1)} %copy-done.13, bf16[160,2048]{1,0:T(8,128)(2,1)} %get-tuple-element.54.refs_2_, ...), custom_call_target="tpu_custom_call" | custom-call | flops 4026531840 | bytes 16777216 | tf_op jit(solution)/shard_map/ffn/pallas_call | solution.py:279
  127.6 9.2 %collective-permute-done.35.refs_3_ = bf16[160,2048]{1,0:T(8,128)(2,1)S(1)} collective-permute-done((bf16[160,2048]{1,0:T(8,128)(2,1)}, bf16[160,2048]{1,0:T(8,128)(2,1)S(1)}, u32[]{:S(2)}, u32[]{:S(2)}) %collective-permute-start.35) | collective-permute-done | bytes 655392 | tf_op jit(solution)/shard_map/ppermute | solution.py:42
  144.4 6.5 %collective-permute-done.34.refs_2_ = bf16[160,2048]{1,0:T(8,128)(2,1)S(1)} collective-permute-done((bf16[160,2048]{1,0:T(8,128)(2,1)}, bf16[160,2048]{1,0:T(8,128)(2,1)S(1)}, u32[]{:S(2)}, u32[]{:S(2)}) %collective-permute-start.34) | collective-permute-done | bytes 655392 | tf_op jit(solution)/shard_map/ppermute | solution.py:42
  157.3 4.0 %unpack.1 = bf16[384,2048]{1,0:T(8,128)(2,1)} custom-call(bf16[384,320]{1,0:T(8,128)(2,1)} %fusion.6.pick_ref, bf16[160,2048]{1,0:T(8,128)(2,1)} %get-tuple-element.56.refs_0_, bf16[160,2048]{1,0:T(8,128)(2,1)} %get-tuple-element.57.refs_1_, bf16[160,2048]{1,0:T(8,128)(2,1)} %copy-done.10, bf16[160,2048]{1,0:T(8,128)(2,1)} %copy-done.8, ...), custom_call_target="tpu_custom_call" | custom-call | tf_op jit(solution)/shard_map/unpack/pallas_call | solution.py:205
  161.3 8.1 %all-to-all-start.1 = ((bf16[16,24,2048]{2,1,0:T(8,128)(2,1)}), bf16[16,24,2048]{2,1,0:T(8,128)(2,1)S(1)}, u32[]{:S(2)}, u32[]{:S(2)}) async-start(bf16[16,24,2048]{2,1,0:T(8,128)(2,1)} %bitcast.13), calls=%async_computation.1 | async-start | bytes 3145728 | tf_op jit(solution)/shard_map/all_to_all | solution.py:319
  169.9 4.8 %own_attention.1 = (f32[1,1024]{1,0:T(1,128)}, f32[1,1024]{1,0:T(1,128)}, f32[128,1024]{1,0:T(8,128)}) custom-call(s32[1024,1]{1,0:T(8,128)} %copy.27.kpos_ref, s32[1,1024]{1,0:T(1,128)} %bitcast.17, bf16[256,1024]{1,0:T(8,128)(2,1)} %get-tuple-element.34.low_ref, bf16[256,1024]{1,0:T(8,128)(2,1)} %get-tuple-element.35.high_ref, ...), custom_call_target="tpu_custom_call" | custom-call | flops 805306368 | bytes 4194304 | tf_op jit(solution)/shard_map/own_attention/pallas_call | solution.py:454
  177.4 20.3 %more_attention.3 = (f32[1,1024]{1,0:T(1,128)}, f32[1,1024]{1,0:T(1,128)}, f32[128,1024]{1,0:T(8,128)}) custom-call(s32[16]{0:T(128)} %compare_convert_fusion.flags_ref, bf16[256,1024]{1,0:T(8,128)(2,1)} %get-tuple-element.34.low_ref, bf16[256,1024]{1,0:T(8,128)(2,1)} %get-tuple-element.35.high_ref, bf16[5120,128]{1,0:T(8,128)(2,1)} %get-tuple-element.37.refs_0_, ...), custom_call_target="tpu_custom_call" | custom-call | flops 1610612736 | bytes 4194304 | tf_op jit(solution)/shard_map/more_attention/pallas_call | solution.py:585
  197.8 12.8 %more_attention.4 = (f32[1,1024]{1,0:T(1,128)}, f32[1,1024]{1,0:T(1,128)}, f32[128,1024]{1,0:T(8,128)}) custom-call(s32[16]{0:T(128)} %compare_convert_fusion.flags_ref, bf16[256,1024]{1,0:T(8,128)(2,1)} %get-tuple-element.34.low_ref, bf16[256,1024]{1,0:T(8,128)(2,1)} %get-tuple-element.35.high_ref, bf16[5120,128]{1,0:T(8,128)(2,1)} %collective-permute-done.10.refs_0_, ...), custom_call_target="tpu_custom_call" | custom-call | flops 3221225472 | bytes 4194304 | tf_op jit(solution)/shard_map/more_attention/pallas_call | solution.py:585
  210.6 26.0 %more_attention.5 = (bf16[128,256]{1,0:T(8,128)(2,1)}, bf16[128,256]{1,0:T(8,128)(2,1)}, bf16[128,256]{1,0:T(8,128)(2,1)}, bf16[128,256]{1,0:T(8,128)(2,1)}) custom-call(s32[16]{0:T(128)} %compare_convert_fusion.flags_ref, bf16[256,1024]{1,0:T(8,128)(2,1)} %get-tuple-element.34.low_ref, bf16[256,1024]{1,0:T(8,128)(2,1)} %get-tuple-element.35.high_ref, ...), custom_call_target="tpu_custom_call" | custom-call | flops 1610612736 | bytes 4194304 | tf_op jit(solution)/shard_map/more_attention/pallas_call | solution.py:585
  238.1 33.9 %collective-permute-start.18 = (bf16[128,256]{1,0:T(8,128)(2,1)}, bf16[128,256]{1,0:T(8,128)(2,1)S(1)}, u32[]{:S(2)}, u32[]{:S(2)}) collective-permute-start(bf16[128,256]{1,0:T(8,128)(2,1)} %get-tuple-element.51), channel_id=1, source_target_pairs={{0,4},{1,5},{2,6},{3,7},{4,0},{5,1},{6,2},{7,3},{8,12},{9,13},{10,... | collective-permute-start | bytes 196616 | tf_op jit(solution)/shard_map/ppermute | solution.py:42
  275.2 4.4 %project.1 = (f32[128,2048]{1,0:T(8,128)}, bf16[128,2048]{1,0:T(8,128)(2,1)}) custom-call(bf16[128,256]{1,0:T(8,128)(2,1)} %get-tuple-element.48.refs_0_, bf16[128,256]{1,0:T(8,128)(2,1)} %copy-done.26, bf16[128,256]{1,0:T(8,128)(2,1)} %copy-done.27, bf16[128,256]{1,0:T(8,128)(2,1)} %copy-done.28, bf16[128,2048]{1,0:T(8,128)(2,1)} %refs_4_.3, ...), custom_call_target="tpu_custom_call" | custom-call | tf_op jit(solution)/shard_map/project/pallas_call | solution.py:613
  281.6 3.1 %combine.1 = bf16[128,2048]{1,0:T(8,128)(2,1)} custom-call(bf16[384,2048]{1,0:T(8,128)(2,1)} %bitcast.14, s32[2,128]{1,0:T(2,128)} %bitcast.19, f32[128,2]{1,0:T(8,128)} %copy.28.w_ref), custom_call_target="tpu_custom_call" | custom-call | tf_op jit(solution)/shard_map/combine/pallas_call | solution.py:148
  (165 shorter events, 70.0 us)
Async XLA Ops:
  11.6 27.4 %all-to-all-start = ((bf16[16,24,2048]{2,1,0:T(8,128)(2,1)}), bf16[16,24,2048]{2,1,0:T(8,128)(2,1)}, u32[]{:S(2)}, u32[]{:S(2)}) async-start(bf16[16,24,2048]{2,1,0:T(8,128)(2,1)} %bitcast.12), calls=%async_computation | async-start | bytes 3145728 | tf_op jit(solution)/shard_map/all_to_all | solution.py:304
  18.0 29.3 %collective-permute-start.25 = (bf16[2,2048,256]{2,1,0:T(8,128)(2,1)S(1)}, bf16[2,2048,256]{2,1,0:T(8,128)(2,1)}, u32[]{:S(2)}, u32[]{:S(2)}) collective-permute-start(bf16[2,2048,256]{2,1,0:T(8,128)(2,1)S(1)} %copy-done), channel_id=1, source_target_pairs={{0,1},{1,0},{2,3},{3,2},{4,5},{5,4},{6,7},{7,6},{8,9},{9,8},{10,11... | collective-permute-start | bytes 6291464 | tf_op jit(solution)/shard_map/ppermute | solution.py:42
  18.7 30.3 %collective-permute-start.26 = (bf16[2,2048,256]{2,1,0:T(8,128)(2,1)}, bf16[2,2048,256]{2,1,0:T(8,128)(2,1)}, u32[]{:S(2)}, u32[]{:S(2)}) collective-permute-start(bf16[2,2048,256]{2,1,0:T(8,128)(2,1)} %refs_5_.3), channel_id=1, source_target_pairs={{0,1},{1,0},{2,3},{3,2},{4,5},{5,4},{6,7},{7,6},{8,9},{9,8},{10,11... | collective-permute-start | bytes 6291464 | tf_op jit(solution)/shard_map/ppermute | solution.py:42
  28.5 36.2 %collective-permute-start.27 = (bf16[2,256,2048]{2,1,0:T(8,128)(2,1)}, bf16[2,256,2048]{2,1,0:T(8,128)(2,1)}, u32[]{:S(2)}, u32[]{:S(2)}) collective-permute-start(bf16[2,256,2048]{2,1,0:T(8,128)(2,1)} %refs_6_.3), channel_id=1, source_target_pairs={{0,1},{1,0},{2,3},{3,2},{4,5},{5,4},{6,7},{7,6},{8,9},{9,8},{10,11... | collective-permute-start | bytes 6291464 | tf_op jit(solution)/shard_map/ppermute | solution.py:42
  47.4 29.6 %collective-permute-start.30 = (bf16[160,2048]{1,0:T(8,128)(2,1)}, bf16[160,2048]{1,0:T(8,128)(2,1)S(1)}, u32[]{:S(2)}, u32[]{:S(2)}) collective-permute-start(bf16[160,2048]{1,0:T(8,128)(2,1)} %get-tuple-element.54.refs_2_), channel_id=1, source_target_pairs={{0,6},{1,7},{2,0},{3,1},{4,2},{5,3},{6,4},{7,5},{8,14},{9,15},{10,... | collective-permute-start | bytes 1966088 | tf_op jit(solution)/shard_map/ppermute | solution.py:42
  48.9 29.5 %collective-permute-start.31 = (bf16[160,2048]{1,0:T(8,128)(2,1)}, bf16[160,2048]{1,0:T(8,128)(2,1)S(1)}, u32[]{:S(2)}, u32[]{:S(2)}) collective-permute-start(bf16[160,2048]{1,0:T(8,128)(2,1)} %get-tuple-element.55.refs_3_), channel_id=1, source_target_pairs={{0,2},{1,3},{2,4},{3,5},{4,6},{5,7},{6,0},{7,1},{8,10},{9,11},{10,... | collective-permute-start | bytes 1966088 | tf_op jit(solution)/shard_map/ppermute | solution.py:42
  58.5 28.1 %collective-permute-start.28 = (bf16[160,2048]{1,0:T(8,128)(2,1)S(1)}, bf16[160,2048]{1,0:T(8,128)(2,1)S(1)}, u32[]{:S(2)}, u32[]{:S(2)}) collective-permute-start(bf16[160,2048]{1,0:T(8,128)(2,1)S(1)} %collective-permute-done.23.refs_0_), channel_id=1, source_target_pairs={{0,2},{1,3},{2,4},{3,5},{4,6},{5,7},{6,0},{7,1},{8,10},{9,11},{10,... | collective-permute-start | bytes 1966088 | tf_op jit(solution)/shard_map/ppermute | solution.py:42
  62.9 28.2 %collective-permute-start.29 = (bf16[160,2048]{1,0:T(8,128)(2,1)S(1)}, bf16[160,2048]{1,0:T(8,128)(2,1)}, u32[]{:S(2)}, u32[]{:S(2)}) collective-permute-start(bf16[160,2048]{1,0:T(8,128)(2,1)S(1)} %collective-permute-done.24.refs_1_), channel_id=1, source_target_pairs={{0,6},{1,7},{2,0},{3,1},{4,2},{5,3},{6,4},{7,5},{8,14},{9,15},{10,... | collective-permute-start | bytes 1966088 | tf_op jit(solution)/shard_map/ppermute | solution.py:42
  64.7 36.6 %collective-permute-start.8 = (bf16[2560,128]{1,0:T(8,128)(2,1)S(1)}, bf16[2560,128]{1,0:T(8,128)(2,1)S(1)}, u32[]{:S(2)}, u32[]{:S(2)}) collective-permute-start(bf16[2560,128]{1,0:T(8,128)(2,1)S(1)} %copy-done.2), channel_id=1, source_target_pairs={{0,96},{1,25},{2,98},{3,27},{4,100},{5,29},{6,102},{7,31},{8,104},... | collective-permute-start | bytes 1966088 | tf_op jit(solution)/shard_map/ppermute | solution.py:42
  76.9 24.4 %collective-permute-start.9 = (bf16[2560,128]{1,0:T(8,128)(2,1)S(1)}, bf16[2560,128]{1,0:T(8,128)(2,1)S(1)}, u32[]{:S(2)}, u32[]{:S(2)}) collective-permute-start(bf16[2560,128]{1,0:T(8,128)(2,1)S(1)} %collective-permute-done.7.b_ref), channel_id=1, source_target_pairs={{0,32},{1,9},{2,34},{3,11},{4,36},{5,13},{6,38},{7,15},{8,40},{9,1... | collective-permute-start | bytes 1966088 | tf_op jit(solution)/shard_map/ppermute | solution.py:42
  106.3 35.5 %collective-permute-start.10 = (bf16[5120,128]{1,0:T(8,128)(2,1)}, bf16[5120,128]{1,0:T(8,128)(2,1)}, u32[]{:S(2)}, u32[]{:S(2)}) collective-permute-start(bf16[5120,128]{1,0:T(8,128)(2,1)} %get-tuple-element.37.refs_0_), channel_id=1, source_target_pairs={{0,8},{1,33},{2,10},{3,35},{4,12},{5,37},{6,14},{7,39},{8,16},{9,4... | collective-permute-start | bytes 3932168 | tf_op jit(solution)/shard_map/ppermute | solution.py:42
  107.8 35.5 %collective-permute-start.12 = (bf16[5120,128]{1,0:T(8,128)(2,1)}, bf16[5120,128]{1,0:T(8,128)(2,1)}, u32[]{:S(2)}, u32[]{:S(2)}) collective-permute-start(bf16[5120,128]{1,0:T(8,128)(2,1)} %get-tuple-element.38.refs_1_), channel_id=1, source_target_pairs={{0,24},{1,97},{2,26},{3,99},{4,28},{5,101},{6,30},{7,103},{8,0},{9... | collective-permute-start | bytes 3932168 | tf_op jit(solution)/shard_map/ppermute | solution.py:42
  127.2 23.7 %collective-permute-start.34 = (bf16[160,2048]{1,0:T(8,128)(2,1)}, bf16[160,2048]{1,0:T(8,128)(2,1)S(1)}, u32[]{:S(2)}, u32[]{:S(2)}) collective-permute-start(bf16[160,2048]{1,0:T(8,128)(2,1)} %get-tuple-element.62), channel_id=1, source_target_pairs={{0,2},{1,3},{2,4},{3,5},{4,6},{5,7},{6,0},{7,1},{8,10},{9,11},{10,... | collective-permute-start | bytes 1966088 | tf_op jit(solution)/shard_map/ppermute | solution.py:42
  136.7 38.0 %collective-permute-start.14 = (bf16[5120,128]{1,0:T(8,128)(2,1)}, bf16[5120,128]{1,0:T(8,128)(2,1)}, u32[]{:S(2)}, u32[]{:S(2)}) collective-permute-start(bf16[5120,128]{1,0:T(8,128)(2,1)} %get-tuple-element.38.refs_1_), channel_id=1, source_target_pairs={{0,8},{1,33},{2,10},{3,35},{4,12},{5,37},{6,14},{7,39},{8,16},{9,4... | collective-permute-start | bytes 3932168 | tf_op jit(solution)/shard_map/ppermute | solution.py:42
  141.7 56.0 %collective-permute-start.15 = (bf16[5120,128]{1,0:T(8,128)(2,1)}, bf16[5120,128]{1,0:T(8,128)(2,1)}, u32[]{:S(2)}, u32[]{:S(2)}) collective-permute-start(bf16[5120,128]{1,0:T(8,128)(2,1)} %get-tuple-element.37.refs_0_), channel_id=1, source_target_pairs={{0,24},{1,97},{2,26},{3,99},{4,28},{5,101},{6,30},{7,103},{8,0},{9... | collective-permute-start | bytes 3932168 | tf_op jit(solution)/shard_map/ppermute | solution.py:42
  143.3 67.3 %collective-permute-start.11 = (bf16[5120,128]{1,0:T(8,128)(2,1)}, bf16[5120,128]{1,0:T(8,128)(2,1)}, u32[]{:S(2)}, u32[]{:S(2)}) collective-permute-start(bf16[5120,128]{1,0:T(8,128)(2,1)} %collective-permute-done.10.refs_0_), channel_id=1, source_target_pairs={{0,8},{1,33},{2,10},{3,35},{4,12},{5,37},{6,14},{7,39},{8,16},{9,4... | collective-permute-start | bytes 3932168 | tf_op jit(solution)/shard_map/ppermute | solution.py:42
  150.9 59.7 %collective-permute-start.13 = (bf16[5120,128]{1,0:T(8,128)(2,1)}, bf16[5120,128]{1,0:T(8,128)(2,1)}, u32[]{:S(2)}, u32[]{:S(2)}) collective-permute-start(bf16[5120,128]{1,0:T(8,128)(2,1)} %collective-permute-done.12.refs_3_), channel_id=1, source_target_pairs={{0,24},{1,97},{2,26},{3,99},{4,28},{5,101},{6,30},{7,103},{8,0},{9... | collective-permute-start | bytes 3932168 | tf_op jit(solution)/shard_map/ppermute | solution.py:42
  153.8 20.9 %collective-permute-start.19 = (bf16[128,2048]{1,0:T(8,128)(2,1)S(1)}, bf16[128,2048]{1,0:T(8,128)(2,1)}, u32[]{:S(2)}, u32[]{:S(2)}) collective-permute-start(bf16[128,2048]{1,0:T(8,128)(2,1)S(1)} %copy-done.17), channel_id=1, source_target_pairs={{0,2},{1,7},{2,4},{3,1},{4,6},{5,3},{6,0},{7,5},{8,10},{9,15},{10,... | collective-permute-start | bytes 1572872 | tf_op jit(solution)/shard_map/ppermute | solution.py:42
  161.3 119.1 %all-to-all-start.1 = ((bf16[16,24,2048]{2,1,0:T(8,128)(2,1)}), bf16[16,24,2048]{2,1,0:T(8,128)(2,1)S(1)}, u32[]{:S(2)}, u32[]{:S(2)}) async-start(bf16[16,24,2048]{2,1,0:T(8,128)(2,1)} %bitcast.13), calls=%async_computation.1 | async-start | bytes 3145728 | tf_op jit(solution)/shard_map/all_to_all | solution.py:319
  174.7 97.3 %collective-permute-start.20 = (bf16[128,2048]{1,0:T(8,128)(2,1)S(1)}, bf16[128,2048]{1,0:T(8,128)(2,1)S(1)}, u32[]{:S(2)}, u32[]{:S(2)}) collective-permute-start(bf16[128,2048]{1,0:T(8,128)(2,1)S(1)} %copy-done.17), channel_id=1, source_target_pairs={{0,6},{1,3},{2,0},{3,5},{4,2},{5,7},{6,4},{7,1},{8,14},{9,11},{10,... | collective-permute-start | bytes 1572872 | tf_op jit(solution)/shard_map/ppermute | solution.py:42
  174.7 97.3 %collective-permute-start.21 = (bf16[128,2048]{1,0:T(8,128)(2,1)}, bf16[128,2048]{1,0:T(8,128)(2,1)S(1)}, u32[]{:S(2)}, u32[]{:S(2)}) collective-permute-start(bf16[128,2048]{1,0:T(8,128)(2,1)} %collective-permute-done.19.refs_5_), channel_id=1, source_target_pairs={{0,2},{1,7},{2,4},{3,1},{4,6},{5,3},{6,0},{7,5},{8,10},{9,15},{10,... | collective-permute-start | bytes 1572872 | tf_op jit(solution)/shard_map/ppermute | solution.py:42
  236.6 35.4 %collective-permute-start.16 = (bf16[128,256]{1,0:T(8,128)(2,1)}, bf16[128,256]{1,0:T(8,128)(2,1)S(1)}, u32[]{:S(2)}, u32[]{:S(2)}) collective-permute-start(bf16[128,256]{1,0:T(8,128)(2,1)} %get-tuple-element.49), channel_id=1, source_target_pairs={{0,2},{1,7},{2,4},{3,1},{4,6},{5,3},{6,0},{7,5},{8,10},{9,15},{10,... | collective-permute-start | bytes 196616 | tf_op jit(solution)/shard_map/ppermute | solution.py:42
  236.7 36.0 %collective-permute-start.17 = (bf16[128,256]{1,0:T(8,128)(2,1)}, bf16[128,256]{1,0:T(8,128)(2,1)S(1)}, u32[]{:S(2)}, u32[]{:S(2)}) collective-permute-start(bf16[128,256]{1,0:T(8,128)(2,1)} %get-tuple-element.50), channel_id=1, source_target_pairs={{0,6},{1,3},{2,0},{3,5},{4,2},{5,7},{6,4},{7,1},{8,14},{9,11},{10,... | collective-permute-start | bytes 196616 | tf_op jit(solution)/shard_map/ppermute | solution.py:42
  238.1 36.4 %collective-permute-start.18 = (bf16[128,256]{1,0:T(8,128)(2,1)}, bf16[128,256]{1,0:T(8,128)(2,1)S(1)}, u32[]{:S(2)}, u32[]{:S(2)}) collective-permute-start(bf16[128,256]{1,0:T(8,128)(2,1)} %get-tuple-element.51), channel_id=1, source_target_pairs={{0,4},{1,5},{2,6},{3,7},{4,0},{5,1},{6,2},{7,3},{8,12},{9,13},{10,... | collective-permute-start | bytes 196616 | tf_op jit(solution)/shard_map/ppermute | solution.py:42
  (51 other events, 675.5 us)
where the time goes:
time: 288 us
  Pallas kernels  116 us (40%)
  starting transfers between devices  89 us (31%)
  waiting for transfers between devices  66.2 us (23%)
  local copies, waits for them, and re-layouts  10.3 us (4%)
  other arithmetic  5.08 us (2%)
    ppermute x38, starting transfers between devices, send(): return lax.ppermute(a, ('ep', 'tp'), pairs(move))  74.4 us
    ppermute x38, waiting for transfers between devices, send(): return lax.ppermute(a, ('ep', 'tp'), pairs(move))  64.4 us
    pallas_call x3, Pallas kernels, more_attention(): pl.pallas_call(functools.partial(more_body, count, first, final), in_spec...  59.1 us
    pallas_call x2, Pallas kernels, ffn(): pl.pallas_call(functools.partial(ffn_body, count), in_specs=[vmem] * 2 *...  20 us
    unnamed x72, local copies, waits for them, and re-layouts  9.2 us
    all_to_all x1, starting transfers between devices, experts_half(): lax.all_to_all(back.reshape(16, CHUNK, width), 'ep', split_axis=0, concat...  8.11 us
    all_to_all x1, starting transfers between devices, experts_half(): lax.all_to_all(outgoing.reshape(16, CHUNK, width), 'ep', split_axis=0, co...  6.48 us
  transfers between devices with their start and end apart: 40, of which 12 were waited for; matrix products, arithmetic and copies ran while one was open for 2% of the time, Pallas kernels for 39%

commit v1 on v0

--- a/solution.py
+++ b/solution.py
@@ -430,8 +430,9 @@
     pieces = [load_piece(kv_ref, k) for k in range(2)]
     lefts = [pieces[0][0], pieces[0][1], pieces[1][0], pieces[1][1]]
     value = jnp.concatenate([pieces[0][2], pieces[1][2]], axis=1)
-    for part in range(low_ref.shape[1] // tile):
-        cols = slice(part * tile, (part + 1) * tile)
+
+    def one(part, _):
+        cols = pl.ds(pl.multiple_of(part * tile, tile), tile)
         scores = []
         for k, left in enumerate(lefts):
             s = dot(left, (high_ref if k % 2 else low_ref)[:, cols])
@@ -445,6 +446,9 @@
         m_ref[:, cols] = m
         l_ref[:, cols] = (sums[0] + sums[1]) + (sums[2] + sums[3])
         acc_ref[:, cols] = dot(value, jnp.concatenate([p.astype(BF) for p in probs], axis=0))
+        return 0
+
+    lax.fori_loop(0, low_ref.shape[1] // tile, one, 0)
 
 
 def own_attention(low, high, kv, positions):
@@ -639,9 +643,10 @@
 
 def sources():
     near = [(d, 0) for d in LINE]
-    wide = [(a, b) for b in (1, -1) for a in LINE]
+    wide = [(a, 1) for a in LINE[:2]] + [(a, -1) for a in LINE[2:]]
+    more = [(a, 1) for a in LINE[2:]] + [(a, -1) for a in LINE[:2]]
     far = [(a, 2) for a in LINE]
-    return near + wide + far
+    return near + wide + more + far
 
 
 def own_block(query_latent, kv_latent, rope_key, query_gain, kv_gain):
@@ -682,7 +687,10 @@
     behind, ahead, far = ring_halves(one, two, along_two)
     state = own_attention(low, high, kv, inside)
     state = more_attention(low, high, (one, two), flags, 0, state)
-    state = more_attention(low, high, (*behind, *ahead), flags, 4, state)
+    wide = behind[0], ahead[1]
+    more = behind[1], ahead[0]
+    state = more_attention(low, high, wide, flags, 4, state)
+    state = more_attention(low, high, more, flags, 8, state)
     attended = more_attention(low, high, far, flags, 12, state, final=True)
     attended = (
         attended[0],

time: 288 us -> 277 us (0.962)
  the two profiles are of different devices: /device:TPU:103 before, /device:TPU:97 now
where the time goes in v1:
time: 277 us; the launch traced here: 276 us
  Pallas kernels  104 us (38%)
  starting transfers between devices  89.4 us (32%)
  waiting for transfers between devices  66 us (24%)
  local copies, waits for them, and re-layouts  10.3 us (4%)
  other arithmetic  5.08 us (2%)
    ppermute x38, starting transfers between devices, send(): return lax.ppermute(a, ('ep', 'tp'), pairs(move))  72.9 us
    ppermute x38, waiting for transfers between devices, send(): return lax.ppermute(a, ('ep', 'tp'), pairs(move))  61.7 us
    pallas_call x4, Pallas kernels, more_attention(): pl.pallas_call(functools.partial(more_body, count, first, final), in_spec...  46.4 us
    pallas_call x2, Pallas kernels, ffn(): pl.pallas_call(functools.partial(ffn_body, count), in_specs=[vmem] * 2 *...  20 us
    all_to_all x1, starting transfers between devices, experts_half(): lax.all_to_all(back.reshape(16, CHUNK, width), 'ep', split_axis=0, concat...  9.96 us
    unnamed x72, local copies, waits for them, and re-layouts  9.14 us
    all_to_all x1, starting transfers between devices, experts_half(): lax.all_to_all(outgoing.reshape(16, CHUNK, width), 'ep', split_axis=0, co...  6.56 us
    pallas_call x1, Pallas kernels, own_attention(): pl.pallas_call(own_body, in_specs=[vmem] * 5, out_specs=[vmem] * 3, out_s...  5.65 us
  transfers between devices with their start and end apart: 40, of which 12 were waited for; matrix products, arithmetic and copies ran while one was open for 2% of the time, Pallas kernels for 36%

profile of v1, /device:TPU:97, one launch (start us, length us, event | category | flops | bytes accessed | tf_op | source)
XLA Modules:
  0.0 276.1 jit_solution(18236235526000089576)
XLA Ops:
  8.4 3.1 %dispatch.1 = bf16[384,2048]{1,0:T(8,128)(2,1)} custom-call(bf16[128,2048]{1,0:T(8,128)(2,1)} %x_ref.1, f32[2048]{0:T(1024)} %gain_ref.1, s32[2,128]{1,0:T(2,128)} %bitcast.18), custom_call_target="tpu_custom_call" | custom-call | tf_op jit(solution)/shard_map/dispatch/pallas_call | solution.py:118
  11.6 6.6 %all-to-all-start = ((bf16[16,24,2048]{2,1,0:T(8,128)(2,1)}), bf16[16,24,2048]{2,1,0:T(8,128)(2,1)}, u32[]{:S(2)}, u32[]{:S(2)}) async-start(bf16[16,24,2048]{2,1,0:T(8,128)(2,1)} %bitcast.12), calls=%async_computation | async-start | bytes 3145728 | tf_op jit(solution)/shard_map/all_to_all | solution.py:304
  21.8 4.2 %collective-permute-done.5.refs_6_ = bf16[128,1536]{1,0:T(8,128)(2,1)} collective-permute-done((bf16[128,1536]{1,0:T(8,128)(2,1)S(1)}, bf16[128,1536]{1,0:T(8,128)(2,1)}, u32[]{:S(2)}, u32[]{:S(2)}) %collective-permute-start.5) | collective-permute-done | bytes 393248 | tf_op jit(solution)/shard_map/ppermute | solution.py:42
  31.4 4.4 %heads.1 = (bf16[2560,128]{1,0:T(8,128)(2,1)}, bf16[256,1024]{1,0:T(8,128)(2,1)}, bf16[256,1024]{1,0:T(8,128)(2,1)}) custom-call(bf16[128,1536]{1,0:T(8,128)(2,1)} %prepare.1.refs_0_, bf16[128,1536]{1,0:T(8,128)(2,1)} %copy-done.23, bf16[128,1536]{1,0:T(8,128)(2,1)} %copy-done.21, bf16[128,1536]{1,0:T(8,128)(2,1)} %copy-done.24, ...), custom_call_target="tpu_custom_call" | custom-call | flops 570425344 | bytes 6291456 | tf_op jit(solution)/shard_map/heads/pallas_call | solution.py:392
  38.3 4.3 %all-to-all-done = bf16[16,24,2048]{2,1,0:T(8,128)(2,1)} async-done(((bf16[16,24,2048]{2,1,0:T(8,128)(2,1)}), bf16[16,24,2048]{2,1,0:T(8,128)(2,1)}, u32[]{:S(2)}, u32[]{:S(2)}) %all-to-all-start) | async-done | bytes 1572896 | tf_op jit(solution)/shard_map/all_to_all | solution.py:304
  42.6 3.0 %pack.1 = (bf16[160,2048]{1,0:T(8,128)(2,1)}, bf16[160,2048]{1,0:T(8,128)(2,1)}) custom-call(bf16[320,384]{1,0:T(8,128)(2,1)} %fusion.14.pick_ref, bf16[384,2048]{1,0:T(8,128)(2,1)} %bitcast.7.x_ref), custom_call_target="tpu_custom_call" | custom-call | tf_op jit(solution)/shard_map/pack/pallas_call | solution.py:183
  50.5 11.0 %collective-permute-done.23.refs_0_ = bf16[160,2048]{1,0:T(8,128)(2,1)S(1)} collective-permute-done((bf16[160,2048]{1,0:T(8,128)(2,1)}, bf16[160,2048]{1,0:T(8,128)(2,1)S(1)}, u32[]{:S(2)}, u32[]{:S(2)}) %collective-permute-start.23) | collective-permute-done | bytes 655392 | tf_op jit(solution)/shard_map/ppermute | solution.py:42
  67.1 11.1 %collective-permute-done.30.refs_2_ = bf16[160,2048]{1,0:T(8,128)(2,1)S(1)} collective-permute-done((bf16[160,2048]{1,0:T(8,128)(2,1)}, bf16[160,2048]{1,0:T(8,128)(2,1)S(1)}, u32[]{:S(2)}, u32[]{:S(2)}) %collective-permute-start.30) | collective-permute-done | bytes 655392 | tf_op jit(solution)/shard_map/ppermute | solution.py:42
  78.2 11.3 %collective-permute-done.28.refs_0_ = bf16[160,2048]{1,0:T(8,128)(2,1)S(1)} collective-permute-done((bf16[160,2048]{1,0:T(8,128)(2,1)S(1)}, bf16[160,2048]{1,0:T(8,128)(2,1)S(1)}, u32[]{:S(2)}, u32[]{:S(2)}) %collective-permute-start.28) | collective-permute-done | bytes 655392 | tf_op jit(solution)/shard_map/ppermute | solution.py:42
  92.3 10.0 %ffn.3 = (bf16[160,2048]{1,0:T(8,128)(2,1)}, bf16[160,2048]{1,0:T(8,128)(2,1)}, bf16[160,2048]{1,0:T(8,128)(2,1)}, bf16[160,2048]{1,0:T(8,128)(2,1)}) custom-call(bf16[160,2048]{1,0:T(8,128)(2,1)} %copy-done.16, bf16[160,2048]{1,0:T(8,128)(2,1)} %collective-permute-done.29.refs_1_, bf16[160,2048]{1,0:T(8,128)(2,1)} %copy-done.14, ...), custom_call_target="tpu_custom_call" | custom-call | flops 4026531840 | bytes 16777216 | tf_op jit(solution)/shard_map/ffn/pallas_call | solution.py:279
  104.2 3.3 %join.1 = (bf16[5120,128]{1,0:T(8,128)(2,1)}, bf16[5120,128]{1,0:T(8,128)(2,1)}) custom-call(bf16[2560,128]{1,0:T(8,128)(2,1)} %get-tuple-element.39.a_ref.kv_ref, bf16[2560,128]{1,0:T(8,128)(2,1)} %copy-done.3, bf16[2560,128]{1,0:T(8,128)(2,1)} %copy-done.5, bf16[2560,128]{1,0:T(8,128)(2,1)} %copy-done.7), custom_call_target="tpu_custom_call" | custom-call | tf_op jit(solution)/shard_map/join/pallas_call | solution.py:413
  111.8 10.0 %ffn.2 = (bf16[160,2048]{1,0:T(8,128)(2,1)}, bf16[160,2048]{1,0:T(8,128)(2,1)}, bf16[160,2048]{1,0:T(8,128)(2,1)}, bf16[160,2048]{1,0:T(8,128)(2,1)}) custom-call(bf16[160,2048]{1,0:T(8,128)(2,1)} %copy-done.12, bf16[160,2048]{1,0:T(8,128)(2,1)} %copy-done.13, bf16[160,2048]{1,0:T(8,128)(2,1)} %get-tuple-element.60.refs_2_, ...), custom_call_target="tpu_custom_call" | custom-call | flops 4026531840 | bytes 16777216 | tf_op jit(solution)/shard_map/ffn/pallas_call | solution.py:279
  128.1 7.7 %collective-permute-done.35.refs_3_ = bf16[160,2048]{1,0:T(8,128)(2,1)S(1)} collective-permute-done((bf16[160,2048]{1,0:T(8,128)(2,1)}, bf16[160,2048]{1,0:T(8,128)(2,1)S(1)}, u32[]{:S(2)}, u32[]{:S(2)}) %collective-permute-start.35) | collective-permute-done | bytes 655392 | tf_op jit(solution)/shard_map/ppermute | solution.py:42
  143.4 6.5 %collective-permute-done.34.refs_2_ = bf16[160,2048]{1,0:T(8,128)(2,1)S(1)} collective-permute-done((bf16[160,2048]{1,0:T(8,128)(2,1)}, bf16[160,2048]{1,0:T(8,128)(2,1)S(1)}, u32[]{:S(2)}, u32[]{:S(2)}) %collective-permute-start.34) | collective-permute-done | bytes 655392 | tf_op jit(solution)/shard_map/ppermute | solution.py:42
  155.7 4.1 %unpack.1 = bf16[384,2048]{1,0:T(8,128)(2,1)} custom-call(bf16[384,320]{1,0:T(8,128)(2,1)} %fusion.6.pick_ref, bf16[160,2048]{1,0:T(8,128)(2,1)} %get-tuple-element.62.refs_0_, bf16[160,2048]{1,0:T(8,128)(2,1)} %get-tuple-element.63.refs_1_, bf16[160,2048]{1,0:T(8,128)(2,1)} %copy-done.10, bf16[160,2048]{1,0:T(8,128)(2,1)} %copy-done.8, ...), custom_call_target="tpu_custom_call" | custom-call | tf_op jit(solution)/shard_map/unpack/pallas_call | solution.py:205
  159.7 10.0 %all-to-all-start.1 = ((bf16[16,24,2048]{2,1,0:T(8,128)(2,1)}), bf16[16,24,2048]{2,1,0:T(8,128)(2,1)S(1)}, u32[]{:S(2)}, u32[]{:S(2)}) async-start(bf16[16,24,2048]{2,1,0:T(8,128)(2,1)} %bitcast.13), calls=%async_computation.1 | async-start | bytes 3145728 | tf_op jit(solution)/shard_map/all_to_all | solution.py:319
  170.2 5.7 %own_attention.1 = (f32[1,1024]{1,0:T(1,128)}, f32[1,1024]{1,0:T(1,128)}, f32[128,1024]{1,0:T(8,128)}) custom-call(s32[1024,1]{1,0:T(8,128)} %copy.27.kpos_ref, s32[1,1024]{1,0:T(1,128)} %bitcast.17, bf16[256,1024]{1,0:T(8,128)(2,1)} %get-tuple-element.37.low_ref, bf16[256,1024]{1,0:T(8,128)(2,1)} %get-tuple-element.38.high_ref, ...), custom_call_target="tpu_custom_call" | custom-call | flops 805306368 | bytes 4194304 | tf_op jit(solution)/shard_map/own_attention/pallas_call | solution.py:458
  178.6 4.0 %more_attention.4 = (f32[1,1024]{1,0:T(1,128)}, f32[1,1024]{1,0:T(1,128)}, f32[128,1024]{1,0:T(8,128)}) custom-call(s32[16]{0:T(128)} %compare_convert_fusion.flags_ref, bf16[256,1024]{1,0:T(8,128)(2,1)} %get-tuple-element.37.low_ref, bf16[256,1024]{1,0:T(8,128)(2,1)} %get-tuple-element.38.high_ref, bf16[5120,128]{1,0:T(8,128)(2,1)} %get-tuple-element.40.refs_0_, ...), custom_call_target="tpu_custom_call" | custom-call | flops 1610612736 | bytes 4194304 | tf_op jit(solution)/shard_map/more_attention/pallas_call | solution.py:589
  182.6 25.9 %more_attention.5 = (f32[1,1024]{1,0:T(1,128)}, f32[1,1024]{1,0:T(1,128)}, f32[128,1024]{1,0:T(8,128)}) custom-call(s32[16]{0:T(128)} %compare_convert_fusion.flags_ref, bf16[256,1024]{1,0:T(8,128)(2,1)} %get-tuple-element.37.low_ref, bf16[256,1024]{1,0:T(8,128)(2,1)} %get-tuple-element.38.high_ref, bf16[5120,128]{1,0:T(8,128)(2,1)} %collective-permute-done.10.refs_0_, ...), custom_call_target="tpu_custom_call" | custom-call | flops 1610612736 | bytes 4194304 | tf_op jit(solution)/shard_map/more_attention/pallas_call | solution.py:589
  208.5 8.2 %more_attention.6 = (f32[1,1024]{1,0:T(1,128)}, f32[1,1024]{1,0:T(1,128)}, f32[128,1024]{1,0:T(8,128)}) custom-call(s32[16]{0:T(128)} %compare_convert_fusion.flags_ref, bf16[256,1024]{1,0:T(8,128)(2,1)} %get-tuple-element.37.low_ref, bf16[256,1024]{1,0:T(8,128)(2,1)} %get-tuple-element.38.high_ref, bf16[5120,128]{1,0:T(8,128)(2,1)} %collective-permute-done.14.refs_0_, ...), custom_call_target="tpu_custom_call" | custom-call | flops 1610612736 | bytes 4194304 | tf_op jit(solution)/shard_map/more_attention/pallas_call | solution.py:589
  216.7 8.3 %more_attention.7 = (bf16[128,256]{1,0:T(8,128)(2,1)}, bf16[128,256]{1,0:T(8,128)(2,1)}, bf16[128,256]{1,0:T(8,128)(2,1)}, bf16[128,256]{1,0:T(8,128)(2,1)}) custom-call(s32[16]{0:T(128)} %compare_convert_fusion.flags_ref, bf16[256,1024]{1,0:T(8,128)(2,1)} %get-tuple-element.37.low_ref, bf16[256,1024]{1,0:T(8,128)(2,1)} %get-tuple-element.38.high_ref, ...), custom_call_target="tpu_custom_call" | custom-call | flops 1610612736 | bytes 4194304 | tf_op jit(solution)/shard_map/more_attention/pallas_call | solution.py:589
  226.6 33.9 %collective-permute-start.18 = (bf16[128,256]{1,0:T(8,128)(2,1)}, bf16[128,256]{1,0:T(8,128)(2,1)S(1)}, u32[]{:S(2)}, u32[]{:S(2)}) collective-permute-start(bf16[128,256]{1,0:T(8,128)(2,1)} %get-tuple-element.57), channel_id=1, source_target_pairs={{0,4},{1,5},{2,6},{3,7},{4,0},{5,1},{6,2},{7,3},{8,12},{9,13},{10,... | collective-permute-start | bytes 196616 | tf_op jit(solution)/shard_map/ppermute | solution.py:42
  263.7 4.5 %project.1 = (f32[128,2048]{1,0:T(8,128)}, bf16[128,2048]{1,0:T(8,128)(2,1)}) custom-call(bf16[128,256]{1,0:T(8,128)(2,1)} %get-tuple-element.54.refs_0_, bf16[128,256]{1,0:T(8,128)(2,1)} %copy-done.26, bf16[128,256]{1,0:T(8,128)(2,1)} %copy-done.27, bf16[128,256]{1,0:T(8,128)(2,1)} %copy-done.28, bf16[128,2048]{1,0:T(8,128)(2,1)} %refs_4_.3, ...), custom_call_target="tpu_custom_call" | custom-call | tf_op jit(solution)/shard_map/project/pallas_call | solution.py:617
  270.1 3.1 %combine.1 = bf16[128,2048]{1,0:T(8,128)(2,1)} custom-call(bf16[384,2048]{1,0:T(8,128)(2,1)} %bitcast.14, s32[2,128]{1,0:T(2,128)} %bitcast.19, f32[128,2]{1,0:T(8,128)} %copy.28.w_ref), custom_call_target="tpu_custom_call" | custom-call | tf_op jit(solution)/shard_map/combine/pallas_call | solution.py:148
  (166 shorter events, 71.0 us)
Async XLA Ops:
  11.6 31.0 %all-to-all-start = ((bf16[16,24,2048]{2,1,0:T(8,128)(2,1)}), bf16[16,24,2048]{2,1,0:T(8,128)(2,1)}, u32[]{:S(2)}, u32[]{:S(2)}) async-start(bf16[16,24,2048]{2,1,0:T(8,128)(2,1)} %bitcast.12), calls=%async_computation | async-start | bytes 3145728 | tf_op jit(solution)/shard_map/all_to_all | solution.py:304
  18.1 30.9 %collective-permute-start.25 = (bf16[2,2048,256]{2,1,0:T(8,128)(2,1)S(1)}, bf16[2,2048,256]{2,1,0:T(8,128)(2,1)}, u32[]{:S(2)}, u32[]{:S(2)}) collective-permute-start(bf16[2,2048,256]{2,1,0:T(8,128)(2,1)S(1)} %copy-done), channel_id=1, source_target_pairs={{0,1},{1,0},{2,3},{3,2},{4,5},{5,4},{6,7},{7,6},{8,9},{9,8},{10,11... | collective-permute-start | bytes 6291464 | tf_op jit(solution)/shard_map/ppermute | solution.py:42
  18.8 30.8 %collective-permute-start.26 = (bf16[2,2048,256]{2,1,0:T(8,128)(2,1)}, bf16[2,2048,256]{2,1,0:T(8,128)(2,1)}, u32[]{:S(2)}, u32[]{:S(2)}) collective-permute-start(bf16[2,2048,256]{2,1,0:T(8,128)(2,1)} %refs_5_.3), channel_id=1, source_target_pairs={{0,1},{1,0},{2,3},{3,2},{4,5},{5,4},{6,7},{7,6},{8,9},{9,8},{10,11... | collective-permute-start | bytes 6291464 | tf_op jit(solution)/shard_map/ppermute | solution.py:42
  28.6 36.7 %collective-permute-start.27 = (bf16[2,256,2048]{2,1,0:T(8,128)(2,1)}, bf16[2,256,2048]{2,1,0:T(8,128)(2,1)}, u32[]{:S(2)}, u32[]{:S(2)}) collective-permute-start(bf16[2,256,2048]{2,1,0:T(8,128)(2,1)} %refs_6_.3), channel_id=1, source_target_pairs={{0,1},{1,0},{2,3},{3,2},{4,5},{5,4},{6,7},{7,6},{8,9},{9,8},{10,11... | collective-permute-start | bytes 6291464 | tf_op jit(solution)/shard_map/ppermute | solution.py:42
  49.0 29.2 %collective-permute-start.30 = (bf16[160,2048]{1,0:T(8,128)(2,1)}, bf16[160,2048]{1,0:T(8,128)(2,1)S(1)}, u32[]{:S(2)}, u32[]{:S(2)}) collective-permute-start(bf16[160,2048]{1,0:T(8,128)(2,1)} %get-tuple-element.60.refs_2_), channel_id=1, source_target_pairs={{0,6},{1,7},{2,0},{3,1},{4,2},{5,3},{6,4},{7,5},{8,14},{9,15},{10,... | collective-permute-start | bytes 1966088 | tf_op jit(solution)/shard_map/ppermute | solution.py:42
  49.5 28.7 %collective-permute-start.31 = (bf16[160,2048]{1,0:T(8,128)(2,1)}, bf16[160,2048]{1,0:T(8,128)(2,1)S(1)}, u32[]{:S(2)}, u32[]{:S(2)}) collective-permute-start(bf16[160,2048]{1,0:T(8,128)(2,1)} %get-tuple-element.61.refs_3_), channel_id=1, source_target_pairs={{0,2},{1,3},{2,4},{3,5},{4,6},{5,7},{6,0},{7,1},{8,10},{9,11},{10,... | collective-permute-start | bytes 1966088 | tf_op jit(solution)/shard_map/ppermute | solution.py:42
  61.5 28.1 %collective-permute-start.28 = (bf16[160,2048]{1,0:T(8,128)(2,1)S(1)}, bf16[160,2048]{1,0:T(8,128)(2,1)S(1)}, u32[]{:S(2)}, u32[]{:S(2)}) collective-permute-start(bf16[160,2048]{1,0:T(8,128)(2,1)S(1)} %collective-permute-done.23.refs_0_), channel_id=1, source_target_pairs={{0,2},{1,3},{2,4},{3,5},{4,6},{5,7},{6,0},{7,1},{8,10},{9,11},{10,... | collective-permute-start | bytes 1966088 | tf_op jit(solution)/shard_map/ppermute | solution.py:42
  64.1 28.2 %collective-permute-start.29 = (bf16[160,2048]{1,0:T(8,128)(2,1)S(1)}, bf16[160,2048]{1,0:T(8,128)(2,1)}, u32[]{:S(2)}, u32[]{:S(2)}) collective-permute-start(bf16[160,2048]{1,0:T(8,128)(2,1)S(1)} %collective-permute-done.24.refs_1_), channel_id=1, source_target_pairs={{0,6},{1,7},{2,0},{3,1},{4,2},{5,3},{6,4},{7,5},{8,14},{9,15},{10,... | collective-permute-start | bytes 1966088 | tf_op jit(solution)/shard_map/ppermute | solution.py:42
  65.2 37.3 %collective-permute-start.8 = (bf16[2560,128]{1,0:T(8,128)(2,1)S(1)}, bf16[2560,128]{1,0:T(8,128)(2,1)S(1)}, u32[]{:S(2)}, u32[]{:S(2)}) collective-permute-start(bf16[2560,128]{1,0:T(8,128)(2,1)S(1)} %copy-done.2), channel_id=1, source_target_pairs={{0,96},{1,25},{2,98},{3,27},{4,100},{5,29},{6,102},{7,31},{8,104},... | collective-permute-start | bytes 1966088 | tf_op jit(solution)/shard_map/ppermute | solution.py:42
  78.2 24.3 %collective-permute-start.9 = (bf16[2560,128]{1,0:T(8,128)(2,1)S(1)}, bf16[2560,128]{1,0:T(8,128)(2,1)S(1)}, u32[]{:S(2)}, u32[]{:S(2)}) collective-permute-start(bf16[2560,128]{1,0:T(8,128)(2,1)S(1)} %collective-permute-done.7.b_ref), channel_id=1, source_target_pairs={{0,32},{1,9},{2,34},{3,11},{4,36},{5,13},{6,38},{7,15},{8,40},{9,1... | collective-permute-start | bytes 1966088 | tf_op jit(solution)/shard_map/ppermute | solution.py:42
  107.5 33.3 %collective-permute-start.10 = (bf16[5120,128]{1,0:T(8,128)(2,1)}, bf16[5120,128]{1,0:T(8,128)(2,1)}, u32[]{:S(2)}, u32[]{:S(2)}) collective-permute-start(bf16[5120,128]{1,0:T(8,128)(2,1)} %get-tuple-element.40.refs_0_), channel_id=1, source_target_pairs={{0,8},{1,33},{2,10},{3,35},{4,12},{5,37},{6,14},{7,39},{8,16},{9,4... | collective-permute-start | bytes 3932168 | tf_op jit(solution)/shard_map/ppermute | solution.py:42
  107.8 34.9 %collective-permute-start.12 = (bf16[5120,128]{1,0:T(8,128)(2,1)}, bf16[5120,128]{1,0:T(8,128)(2,1)}, u32[]{:S(2)}, u32[]{:S(2)}) collective-permute-start(bf16[5120,128]{1,0:T(8,128)(2,1)} %get-tuple-element.41.refs_1_), channel_id=1, source_target_pairs={{0,24},{1,97},{2,26},{3,99},{4,28},{5,101},{6,30},{7,103},{8,0},{9... | collective-permute-start | bytes 3932168 | tf_op jit(solution)/shard_map/ppermute | solution.py:42
  128.1 21.8 %collective-permute-start.34 = (bf16[160,2048]{1,0:T(8,128)(2,1)}, bf16[160,2048]{1,0:T(8,128)(2,1)S(1)}, u32[]{:S(2)}, u32[]{:S(2)}) collective-permute-start(bf16[160,2048]{1,0:T(8,128)(2,1)} %get-tuple-element.68), channel_id=1, source_target_pairs={{0,2},{1,3},{2,4},{3,5},{4,6},{5,7},{6,0},{7,1},{8,10},{9,11},{10,... | collective-permute-start | bytes 1966088 | tf_op jit(solution)/shard_map/ppermute | solution.py:42
  135.7 40.1 %collective-permute-start.14 = (bf16[5120,128]{1,0:T(8,128)(2,1)}, bf16[5120,128]{1,0:T(8,128)(2,1)}, u32[]{:S(2)}, u32[]{:S(2)}) collective-permute-start(bf16[5120,128]{1,0:T(8,128)(2,1)} %get-tuple-element.41.refs_1_), channel_id=1, source_target_pairs={{0,8},{1,33},{2,10},{3,35},{4,12},{5,37},{6,14},{7,39},{8,16},{9,4... | collective-permute-start | bytes 3932168 | tf_op jit(solution)/shard_map/ppermute | solution.py:42
  140.7 67.7 %collective-permute-start.15 = (bf16[5120,128]{1,0:T(8,128)(2,1)}, bf16[5120,128]{1,0:T(8,128)(2,1)}, u32[]{:S(2)}, u32[]{:S(2)}) collective-permute-start(bf16[5120,128]{1,0:T(8,128)(2,1)} %get-tuple-element.40.refs_0_), channel_id=1, source_target_pairs={{0,24},{1,97},{2,26},{3,99},{4,28},{5,101},{6,30},{7,103},{8,0},{9... | collective-permute-start | bytes 3932168 | tf_op jit(solution)/shard_map/ppermute | solution.py:42
  142.8 74.0 %collective-permute-start.11 = (bf16[5120,128]{1,0:T(8,128)(2,1)}, bf16[5120,128]{1,0:T(8,128)(2,1)}, u32[]{:S(2)}, u32[]{:S(2)}) collective-permute-start(bf16[5120,128]{1,0:T(8,128)(2,1)} %collective-permute-done.10.refs_0_), channel_id=1, source_target_pairs={{0,8},{1,33},{2,10},{3,35},{4,12},{5,37},{6,14},{7,39},{8,16},{9,4... | collective-permute-start | bytes 3932168 | tf_op jit(solution)/shard_map/ppermute | solution.py:42
  149.9 66.8 %collective-permute-start.13 = (bf16[5120,128]{1,0:T(8,128)(2,1)}, bf16[5120,128]{1,0:T(8,128)(2,1)}, u32[]{:S(2)}, u32[]{:S(2)}) collective-permute-start(bf16[5120,128]{1,0:T(8,128)(2,1)} %collective-permute-done.12.refs_1_), channel_id=1, source_target_pairs={{0,24},{1,97},{2,26},{3,99},{4,28},{5,101},{6,30},{7,103},{8,0},{9... | collective-permute-start | bytes 3932168 | tf_op jit(solution)/shard_map/ppermute | solution.py:42
  152.9 22.9 %collective-permute-start.19 = (bf16[128,2048]{1,0:T(8,128)(2,1)S(1)}, bf16[128,2048]{1,0:T(8,128)(2,1)}, u32[]{:S(2)}, u32[]{:S(2)}) collective-permute-start(bf16[128,2048]{1,0:T(8,128)(2,1)S(1)} %copy-done.17), channel_id=1, source_target_pairs={{0,2},{1,7},{2,4},{3,1},{4,6},{5,3},{6,0},{7,5},{8,10},{9,15},{10,... | collective-permute-start | bytes 1572872 | tf_op jit(solution)/shard_map/ppermute | solution.py:42
  159.7 109.2 %all-to-all-start.1 = ((bf16[16,24,2048]{2,1,0:T(8,128)(2,1)}), bf16[16,24,2048]{2,1,0:T(8,128)(2,1)S(1)}, u32[]{:S(2)}, u32[]{:S(2)}) async-start(bf16[16,24,2048]{2,1,0:T(8,128)(2,1)} %bitcast.13), calls=%async_computation.1 | async-start | bytes 3145728 | tf_op jit(solution)/shard_map/all_to_all | solution.py:319
  175.9 84.6 %collective-permute-start.20 = (bf16[128,2048]{1,0:T(8,128)(2,1)S(1)}, bf16[128,2048]{1,0:T(8,128)(2,1)S(1)}, u32[]{:S(2)}, u32[]{:S(2)}) collective-permute-start(bf16[128,2048]{1,0:T(8,128)(2,1)S(1)} %copy-done.17), channel_id=1, source_target_pairs={{0,6},{1,3},{2,0},{3,5},{4,2},{5,7},{6,4},{7,1},{8,14},{9,11},{10,... | collective-permute-start | bytes 1572872 | tf_op jit(solution)/shard_map/ppermute | solution.py:42
  175.9 84.6 %collective-permute-start.21 = (bf16[128,2048]{1,0:T(8,128)(2,1)}, bf16[128,2048]{1,0:T(8,128)(2,1)S(1)}, u32[]{:S(2)}, u32[]{:S(2)}) collective-permute-start(bf16[128,2048]{1,0:T(8,128)(2,1)} %collective-permute-done.19.refs_5_), channel_id=1, source_target_pairs={{0,2},{1,7},{2,4},{3,1},{4,6},{5,3},{6,0},{7,5},{8,10},{9,15},{10,... | collective-permute-start | bytes 1572872 | tf_op jit(solution)/shard_map/ppermute | solution.py:42
  225.1 35.5 %collective-permute-start.16 = (bf16[128,256]{1,0:T(8,128)(2,1)}, bf16[128,256]{1,0:T(8,128)(2,1)S(1)}, u32[]{:S(2)}, u32[]{:S(2)}) collective-permute-start(bf16[128,256]{1,0:T(8,128)(2,1)} %get-tuple-element.55), channel_id=1, source_target_pairs={{0,2},{1,7},{2,4},{3,1},{4,6},{5,3},{6,0},{7,5},{8,10},{9,15},{10,... | collective-permute-start | bytes 196616 | tf_op jit(solution)/shard_map/ppermute | solution.py:42
  225.2 36.0 %collective-permute-start.17 = (bf16[128,256]{1,0:T(8,128)(2,1)}, bf16[128,256]{1,0:T(8,128)(2,1)S(1)}, u32[]{:S(2)}, u32[]{:S(2)}) collective-permute-start(bf16[128,256]{1,0:T(8,128)(2,1)} %get-tuple-element.56), channel_id=1, source_target_pairs={{0,6},{1,3},{2,0},{3,5},{4,2},{5,7},{6,4},{7,1},{8,14},{9,11},{10,... | collective-permute-start | bytes 196616 | tf_op jit(solution)/shard_map/ppermute | solution.py:42
  226.6 36.5 %collective-permute-start.18 = (bf16[128,256]{1,0:T(8,128)(2,1)}, bf16[128,256]{1,0:T(8,128)(2,1)S(1)}, u32[]{:S(2)}, u32[]{:S(2)}) collective-permute-start(bf16[128,256]{1,0:T(8,128)(2,1)} %get-tuple-element.57), channel_id=1, source_target_pairs={{0,4},{1,5},{2,6},{3,7},{4,0},{5,1},{6,2},{7,3},{8,12},{9,13},{10,... | collective-permute-start | bytes 196616 | tf_op jit(solution)/shard_map/ppermute | solution.py:42
  (51 other events, 675.5 us)

commit v2 on v1

--- a/solution.py
+++ b/solution.py
@@ -688,10 +688,9 @@
     state = own_attention(low, high, kv, inside)
     state = more_attention(low, high, (one, two), flags, 0, state)
     wide = behind[0], ahead[1]
-    more = behind[1], ahead[0]
+    rest = behind[1], ahead[0], *far
     state = more_attention(low, high, wide, flags, 4, state)
-    state = more_attention(low, high, more, flags, 8, state)
-    attended = more_attention(low, high, far, flags, 12, state, final=True)
+    attended = more_attention(low, high, rest, flags, 8, state, final=True)
     attended = (
         attended[0],
         send(attended[2], along_y(1)),

time: 277 us -> 290 us (1.047)
  the two profiles are of different devices: /device:TPU:97 before, /device:TPU:103 now
where the time goes in v2:
time: 290 us; the launch traced here: 289 us
  Pallas kernels  135 us (47%)
  starting transfers between devices  71.5 us (25%)
  waiting for transfers between devices  66.3 us (23%)
  local copies, waits for them, and re-layouts  10.2 us (4%)
  other arithmetic  5.08 us (2%)
    pallas_call x3, Pallas kernels, more_attention(): pl.pallas_call(functools.partial(more_body, count, first, final), in_spec...  76.9 us
    ppermute x38, waiting for transfers between devices, send(): return lax.ppermute(a, ('ep', 'tp'), pairs(move))  64.6 us
    ppermute x38, starting transfers between devices, send(): return lax.ppermute(a, ('ep', 'tp'), pairs(move))  57 us
    pallas_call x2, Pallas kernels, ffn(): pl.pallas_call(functools.partial(ffn_body, count), in_specs=[vmem] * 2 *...  20 us
    unnamed x72, local copies, waits for them, and re-layouts  9.13 us
    all_to_all x1, starting transfers between devices, experts_half(): lax.all_to_all(back.reshape(16, CHUNK, width), 'ep', split_axis=0, concat...  7.94 us
    all_to_all x1, starting transfers between devices, experts_half(): lax.all_to_all(outgoing.reshape(16, CHUNK, width), 'ep', split_axis=0, co...  6.48 us
  transfers between devices with their start and end apart: 40, of which 13 were waited for; matrix products, arithmetic and copies ran while one was open for 2% of the time, Pallas kernels for 45%

profile of v2, /device:TPU:103, one launch (start us, length us, event | category | flops | bytes accessed | tf_op | source)
XLA Modules:
  0.0 288.7 jit_solution(10300848431372208167)
XLA Ops:
  8.4 3.1 %dispatch.1 = bf16[384,2048]{1,0:T(8,128)(2,1)} custom-call(bf16[128,2048]{1,0:T(8,128)(2,1)} %x_ref.1, f32[2048]{0:T(1024)} %gain_ref.1, s32[2,128]{1,0:T(2,128)} %bitcast.18), custom_call_target="tpu_custom_call" | custom-call | tf_op jit(solution)/shard_map/dispatch/pallas_call | solution.py:118
  11.6 6.5 %all-to-all-start = ((bf16[16,24,2048]{2,1,0:T(8,128)(2,1)}), bf16[16,24,2048]{2,1,0:T(8,128)(2,1)}, u32[]{:S(2)}, u32[]{:S(2)}) async-start(bf16[16,24,2048]{2,1,0:T(8,128)(2,1)} %bitcast.12), calls=%async_computation | async-start | bytes 3145728 | tf_op jit(solution)/shard_map/all_to_all | solution.py:304
  21.7 4.2 %collective-permute-done.5.refs_6_ = bf16[128,1536]{1,0:T(8,128)(2,1)} collective-permute-done((bf16[128,1536]{1,0:T(8,128)(2,1)S(1)}, bf16[128,1536]{1,0:T(8,128)(2,1)}, u32[]{:S(2)}, u32[]{:S(2)}) %collective-permute-start.5) | collective-permute-done | bytes 393248 | tf_op jit(solution)/shard_map/ppermute | solution.py:42
  31.3 4.4 %heads.1 = (bf16[2560,128]{1,0:T(8,128)(2,1)}, bf16[256,1024]{1,0:T(8,128)(2,1)}, bf16[256,1024]{1,0:T(8,128)(2,1)}) custom-call(bf16[128,1536]{1,0:T(8,128)(2,1)} %prepare.1.refs_0_, bf16[128,1536]{1,0:T(8,128)(2,1)} %copy-done.23, bf16[128,1536]{1,0:T(8,128)(2,1)} %copy-done.21, bf16[128,1536]{1,0:T(8,128)(2,1)} %copy-done.24, ...), custom_call_target="tpu_custom_call" | custom-call | flops 570425344 | bytes 6291456 | tf_op jit(solution)/shard_map/heads/pallas_call | solution.py:392
  42.1 4.6 %collective-permute-done.7.b_ref = bf16[2560,128]{1,0:T(8,128)(2,1)S(1)} collective-permute-done((bf16[2560,128]{1,0:T(8,128)(2,1)}, bf16[2560,128]{1,0:T(8,128)(2,1)S(1)}, u32[]{:S(2)}, u32[]{:S(2)}) %collective-permute-start.7) | collective-permute-done | bytes 655392 | tf_op jit(solution)/shard_map/ppermute | solution.py:42
  48.9 9.6 %collective-permute-done.23.refs_0_ = bf16[160,2048]{1,0:T(8,128)(2,1)S(1)} collective-permute-done((bf16[160,2048]{1,0:T(8,128)(2,1)}, bf16[160,2048]{1,0:T(8,128)(2,1)S(1)}, u32[]{:S(2)}, u32[]{:S(2)}) %collective-permute-start.23) | collective-permute-done | bytes 655392 | tf_op jit(solution)/shard_map/ppermute | solution.py:42
  58.5 4.3 %collective-permute-done.24.refs_1_ = bf16[160,2048]{1,0:T(8,128)(2,1)S(1)} collective-permute-done((bf16[160,2048]{1,0:T(8,128)(2,1)}, bf16[160,2048]{1,0:T(8,128)(2,1)S(1)}, u32[]{:S(2)}, u32[]{:S(2)}) %collective-permute-start.24) | collective-permute-done | bytes 655392 | tf_op jit(solution)/shard_map/ppermute | solution.py:42
  65.1 11.7 %collective-permute-done.30.refs_2_ = bf16[160,2048]{1,0:T(8,128)(2,1)S(1)} collective-permute-done((bf16[160,2048]{1,0:T(8,128)(2,1)}, bf16[160,2048]{1,0:T(8,128)(2,1)S(1)}, u32[]{:S(2)}, u32[]{:S(2)}) %collective-permute-start.30) | collective-permute-done | bytes 655392 | tf_op jit(solution)/shard_map/ppermute | solution.py:42
  78.4 8.2 %collective-permute-done.28.refs_0_ = bf16[160,2048]{1,0:T(8,128)(2,1)S(1)} collective-permute-done((bf16[160,2048]{1,0:T(8,128)(2,1)S(1)}, bf16[160,2048]{1,0:T(8,128)(2,1)S(1)}, u32[]{:S(2)}, u32[]{:S(2)}) %collective-permute-start.28) | collective-permute-done | bytes 655392 | tf_op jit(solution)/shard_map/ppermute | solution.py:42
  87.5 3.5 %collective-permute-done.29.refs_1_ = bf16[160,2048]{1,0:T(8,128)(2,1)} collective-permute-done((bf16[160,2048]{1,0:T(8,128)(2,1)S(1)}, bf16[160,2048]{1,0:T(8,128)(2,1)}, u32[]{:S(2)}, u32[]{:S(2)}) %collective-permute-start.29) | collective-permute-done | bytes 655392 | tf_op jit(solution)/shard_map/ppermute | solution.py:42
  91.0 10.0 %ffn.3 = (bf16[160,2048]{1,0:T(8,128)(2,1)}, bf16[160,2048]{1,0:T(8,128)(2,1)}, bf16[160,2048]{1,0:T(8,128)(2,1)}, bf16[160,2048]{1,0:T(8,128)(2,1)}) custom-call(bf16[160,2048]{1,0:T(8,128)(2,1)} %copy-done.16, bf16[160,2048]{1,0:T(8,128)(2,1)} %collective-permute-done.29.refs_1_, bf16[160,2048]{1,0:T(8,128)(2,1)} %copy-done.14, ...), custom_call_target="tpu_custom_call" | custom-call | flops 4026531840 | bytes 16777216 | tf_op jit(solution)/shard_map/ffn/pallas_call | solution.py:279
  103.0 3.3 %join.1 = (bf16[5120,128]{1,0:T(8,128)(2,1)}, bf16[5120,128]{1,0:T(8,128)(2,1)}) custom-call(bf16[2560,128]{1,0:T(8,128)(2,1)} %get-tuple-element.36.a_ref.kv_ref, bf16[2560,128]{1,0:T(8,128)(2,1)} %copy-done.3, bf16[2560,128]{1,0:T(8,128)(2,1)} %copy-done.5, bf16[2560,128]{1,0:T(8,128)(2,1)} %copy-done.7), custom_call_target="tpu_custom_call" | custom-call | tf_op jit(solution)/shard_map/join/pallas_call | solution.py:413
  111.0 10.0 %ffn.2 = (bf16[160,2048]{1,0:T(8,128)(2,1)}, bf16[160,2048]{1,0:T(8,128)(2,1)}, bf16[160,2048]{1,0:T(8,128)(2,1)}, bf16[160,2048]{1,0:T(8,128)(2,1)}) custom-call(bf16[160,2048]{1,0:T(8,128)(2,1)} %copy-done.12, bf16[160,2048]{1,0:T(8,128)(2,1)} %copy-done.13, bf16[160,2048]{1,0:T(8,128)(2,1)} %get-tuple-element.54.refs_2_, ...), custom_call_target="tpu_custom_call" | custom-call | flops 4026531840 | bytes 16777216 | tf_op jit(solution)/shard_map/ffn/pallas_call | solution.py:279
  127.6 9.3 %collective-permute-done.35.refs_3_ = bf16[160,2048]{1,0:T(8,128)(2,1)S(1)} collective-permute-done((bf16[160,2048]{1,0:T(8,128)(2,1)}, bf16[160,2048]{1,0:T(8,128)(2,1)S(1)}, u32[]{:S(2)}, u32[]{:S(2)}) %collective-permute-start.35) | collective-permute-done | bytes 655392 | tf_op jit(solution)/shard_map/ppermute | solution.py:42
  144.6 6.5 %collective-permute-done.34.refs_2_ = bf16[160,2048]{1,0:T(8,128)(2,1)S(1)} collective-permute-done((bf16[160,2048]{1,0:T(8,128)(2,1)}, bf16[160,2048]{1,0:T(8,128)(2,1)S(1)}, u32[]{:S(2)}, u32[]{:S(2)}) %collective-permute-start.34) | collective-permute-done | bytes 655392 | tf_op jit(solution)/shard_map/ppermute | solution.py:42
  157.5 4.0 %unpack.1 = bf16[384,2048]{1,0:T(8,128)(2,1)} custom-call(bf16[384,320]{1,0:T(8,128)(2,1)} %fusion.6.pick_ref, bf16[160,2048]{1,0:T(8,128)(2,1)} %get-tuple-element.56.refs_0_, bf16[160,2048]{1,0:T(8,128)(2,1)} %get-tuple-element.57.refs_1_, bf16[160,2048]{1,0:T(8,128)(2,1)} %copy-done.10, bf16[160,2048]{1,0:T(8,128)(2,1)} %copy-done.8, ...), custom_call_target="tpu_custom_call" | custom-call | tf_op jit(solution)/shard_map/unpack/pallas_call | solution.py:205
  161.6 7.9 %all-to-all-start.1 = ((bf16[16,24,2048]{2,1,0:T(8,128)(2,1)}), bf16[16,24,2048]{2,1,0:T(8,128)(2,1)S(1)}, u32[]{:S(2)}, u32[]{:S(2)}) async-start(bf16[16,24,2048]{2,1,0:T(8,128)(2,1)} %bitcast.13), calls=%async_computation.1 | async-start | bytes 3145728 | tf_op jit(solution)/shard_map/all_to_all | solution.py:319
  170.1 5.7 %own_attention.1 = (f32[1,1024]{1,0:T(1,128)}, f32[1,1024]{1,0:T(1,128)}, f32[128,1024]{1,0:T(8,128)}) custom-call(s32[1024,1]{1,0:T(8,128)} %copy.27.kpos_ref, s32[1,1024]{1,0:T(1,128)} %bitcast.17, bf16[256,1024]{1,0:T(8,128)(2,1)} %get-tuple-element.34.low_ref, bf16[256,1024]{1,0:T(8,128)(2,1)} %get-tuple-element.35.high_ref, ...), custom_call_target="tpu_custom_call" | custom-call | flops 805306368 | bytes 4194304 | tf_op jit(solution)/shard_map/own_attention/pallas_call | solution.py:458
  178.4 20.3 %more_attention.3 = (f32[1,1024]{1,0:T(1,128)}, f32[1,1024]{1,0:T(1,128)}, f32[128,1024]{1,0:T(8,128)}) custom-call(s32[16]{0:T(128)} %compare_convert_fusion.flags_ref, bf16[256,1024]{1,0:T(8,128)(2,1)} %get-tuple-element.34.low_ref, bf16[256,1024]{1,0:T(8,128)(2,1)} %get-tuple-element.35.high_ref, bf16[5120,128]{1,0:T(8,128)(2,1)} %get-tuple-element.38.refs_0_, ...), custom_call_target="tpu_custom_call" | custom-call | flops 1610612736 | bytes 4194304 | tf_op jit(solution)/shard_map/more_attention/pallas_call | solution.py:589
  198.7 8.2 %more_attention.4 = (f32[1,1024]{1,0:T(1,128)}, f32[1,1024]{1,0:T(1,128)}, f32[128,1024]{1,0:T(8,128)}) custom-call(s32[16]{0:T(128)} %compare_convert_fusion.flags_ref, bf16[256,1024]{1,0:T(8,128)(2,1)} %get-tuple-element.34.low_ref, bf16[256,1024]{1,0:T(8,128)(2,1)} %get-tuple-element.35.high_ref, bf16[5120,128]{1,0:T(8,128)(2,1)} %collective-permute-done.12.refs_0_, ...), custom_call_target="tpu_custom_call" | custom-call | flops 1610612736 | bytes 4194304 | tf_op jit(solution)/shard_map/more_attention/pallas_call | solution.py:589
  207.0 48.4 %more_attention.5 = (bf16[128,256]{1,0:T(8,128)(2,1)}, bf16[128,256]{1,0:T(8,128)(2,1)}, bf16[128,256]{1,0:T(8,128)(2,1)}, bf16[128,256]{1,0:T(8,128)(2,1)}) custom-call(s32[16]{0:T(128)} %compare_convert_fusion.flags_ref, bf16[256,1024]{1,0:T(8,128)(2,1)} %get-tuple-element.34.low_ref, bf16[256,1024]{1,0:T(8,128)(2,1)} %get-tuple-element.35.high_ref, ...), custom_call_target="tpu_custom_call" | custom-call | flops 3221225472 | bytes 4194304 | tf_op jit(solution)/shard_map/more_attention/pallas_call | solution.py:589
  256.9 16.2 %collective-permute-start.18 = (bf16[128,256]{1,0:T(8,128)(2,1)}, bf16[128,256]{1,0:T(8,128)(2,1)S(1)}, u32[]{:S(2)}, u32[]{:S(2)}) collective-permute-start(bf16[128,256]{1,0:T(8,128)(2,1)} %get-tuple-element.51), channel_id=1, source_target_pairs={{0,4},{1,5},{2,6},{3,7},{4,0},{5,1},{6,2},{7,3},{8,12},{9,13},{10,... | collective-permute-start | bytes 196616 | tf_op jit(solution)/shard_map/ppermute | solution.py:42
  276.4 4.4 %project.1 = (f32[128,2048]{1,0:T(8,128)}, bf16[128,2048]{1,0:T(8,128)(2,1)}) custom-call(bf16[128,256]{1,0:T(8,128)(2,1)} %get-tuple-element.48.refs_0_, bf16[128,256]{1,0:T(8,128)(2,1)} %copy-done.26, bf16[128,256]{1,0:T(8,128)(2,1)} %copy-done.27, bf16[128,256]{1,0:T(8,128)(2,1)} %copy-done.28, bf16[128,2048]{1,0:T(8,128)(2,1)} %refs_4_.3, ...), custom_call_target="tpu_custom_call" | custom-call | tf_op jit(solution)/shard_map/project/pallas_call | solution.py:617
  282.7 3.1 %combine.1 = bf16[128,2048]{1,0:T(8,128)(2,1)} custom-call(bf16[384,2048]{1,0:T(8,128)(2,1)} %bitcast.14, s32[2,128]{1,0:T(2,128)} %bitcast.19, f32[128,2]{1,0:T(8,128)} %copy.28.w_ref), custom_call_target="tpu_custom_call" | custom-call | tf_op jit(solution)/shard_map/combine/pallas_call | solution.py:148
  (165 shorter events, 70.2 us)
Async XLA Ops:
  11.6 27.4 %all-to-all-start = ((bf16[16,24,2048]{2,1,0:T(8,128)(2,1)}), bf16[16,24,2048]{2,1,0:T(8,128)(2,1)}, u32[]{:S(2)}, u32[]{:S(2)}) async-start(bf16[16,24,2048]{2,1,0:T(8,128)(2,1)} %bitcast.12), calls=%async_computation | async-start | bytes 3145728 | tf_op jit(solution)/shard_map/all_to_all | solution.py:304
  18.0 29.3 %collective-permute-start.25 = (bf16[2,2048,256]{2,1,0:T(8,128)(2,1)S(1)}, bf16[2,2048,256]{2,1,0:T(8,128)(2,1)}, u32[]{:S(2)}, u32[]{:S(2)}) collective-permute-start(bf16[2,2048,256]{2,1,0:T(8,128)(2,1)S(1)} %copy-done), channel_id=1, source_target_pairs={{0,1},{1,0},{2,3},{3,2},{4,5},{5,4},{6,7},{7,6},{8,9},{9,8},{10,11... | collective-permute-start | bytes 6291464 | tf_op jit(solution)/shard_map/ppermute | solution.py:42
  18.7 30.3 %collective-permute-start.26 = (bf16[2,2048,256]{2,1,0:T(8,128)(2,1)}, bf16[2,2048,256]{2,1,0:T(8,128)(2,1)}, u32[]{:S(2)}, u32[]{:S(2)}) collective-permute-start(bf16[2,2048,256]{2,1,0:T(8,128)(2,1)} %refs_5_.3), channel_id=1, source_target_pairs={{0,1},{1,0},{2,3},{3,2},{4,5},{5,4},{6,7},{7,6},{8,9},{9,8},{10,11... | collective-permute-start | bytes 6291464 | tf_op jit(solution)/shard_map/ppermute | solution.py:42
  28.5 36.1 %collective-permute-start.27 = (bf16[2,256,2048]{2,1,0:T(8,128)(2,1)}, bf16[2,256,2048]{2,1,0:T(8,128)(2,1)}, u32[]{:S(2)}, u32[]{:S(2)}) collective-permute-start(bf16[2,256,2048]{2,1,0:T(8,128)(2,1)} %refs_6_.3), channel_id=1, source_target_pairs={{0,1},{1,0},{2,3},{3,2},{4,5},{5,4},{6,7},{7,6},{8,9},{9,8},{10,11... | collective-permute-start | bytes 6291464 | tf_op jit(solution)/shard_map/ppermute | solution.py:42
  47.4 29.5 %collective-permute-start.30 = (bf16[160,2048]{1,0:T(8,128)(2,1)}, bf16[160,2048]{1,0:T(8,128)(2,1)S(1)}, u32[]{:S(2)}, u32[]{:S(2)}) collective-permute-start(bf16[160,2048]{1,0:T(8,128)(2,1)} %get-tuple-element.54.refs_2_), channel_id=1, source_target_pairs={{0,6},{1,7},{2,0},{3,1},{4,2},{5,3},{6,4},{7,5},{8,14},{9,15},{10,... | collective-permute-start | bytes 1966088 | tf_op jit(solution)/shard_map/ppermute | solution.py:42
  48.9 29.5 %collective-permute-start.31 = (bf16[160,2048]{1,0:T(8,128)(2,1)}, bf16[160,2048]{1,0:T(8,128)(2,1)S(1)}, u32[]{:S(2)}, u32[]{:S(2)}) collective-permute-start(bf16[160,2048]{1,0:T(8,128)(2,1)} %get-tuple-element.55.refs_3_), channel_id=1, source_target_pairs={{0,2},{1,3},{2,4},{3,5},{4,6},{5,7},{6,0},{7,1},{8,10},{9,11},{10,... | collective-permute-start | bytes 1966088 | tf_op jit(solution)/shard_map/ppermute | solution.py:42
  58.5 28.1 %collective-permute-start.28 = (bf16[160,2048]{1,0:T(8,128)(2,1)S(1)}, bf16[160,2048]{1,0:T(8,128)(2,1)S(1)}, u32[]{:S(2)}, u32[]{:S(2)}) collective-permute-start(bf16[160,2048]{1,0:T(8,128)(2,1)S(1)} %collective-permute-done.23.refs_0_), channel_id=1, source_target_pairs={{0,2},{1,3},{2,4},{3,5},{4,6},{5,7},{6,0},{7,1},{8,10},{9,11},{10,... | collective-permute-start | bytes 1966088 | tf_op jit(solution)/shard_map/ppermute | solution.py:42
  62.8 28.2 %collective-permute-start.29 = (bf16[160,2048]{1,0:T(8,128)(2,1)S(1)}, bf16[160,2048]{1,0:T(8,128)(2,1)}, u32[]{:S(2)}, u32[]{:S(2)}) collective-permute-start(bf16[160,2048]{1,0:T(8,128)(2,1)S(1)} %collective-permute-done.24.refs_1_), channel_id=1, source_target_pairs={{0,6},{1,7},{2,0},{3,1},{4,2},{5,3},{6,4},{7,5},{8,14},{9,15},{10,... | collective-permute-start | bytes 1966088 | tf_op jit(solution)/shard_map/ppermute | solution.py:42
  64.6 36.7 %collective-permute-start.8 = (bf16[2560,128]{1,0:T(8,128)(2,1)S(1)}, bf16[2560,128]{1,0:T(8,128)(2,1)S(1)}, u32[]{:S(2)}, u32[]{:S(2)}) collective-permute-start(bf16[2560,128]{1,0:T(8,128)(2,1)S(1)} %copy-done.2), channel_id=1, source_target_pairs={{0,96},{1,25},{2,98},{3,27},{4,100},{5,29},{6,102},{7,31},{8,104},... | collective-permute-start | bytes 1966088 | tf_op jit(solution)/shard_map/ppermute | solution.py:42
  76.8 24.5 %collective-permute-start.9 = (bf16[2560,128]{1,0:T(8,128)(2,1)S(1)}, bf16[2560,128]{1,0:T(8,128)(2,1)S(1)}, u32[]{:S(2)}, u32[]{:S(2)}) collective-permute-start(bf16[2560,128]{1,0:T(8,128)(2,1)S(1)} %collective-permute-done.7.b_ref), channel_id=1, source_target_pairs={{0,32},{1,9},{2,34},{3,11},{4,36},{5,13},{6,38},{7,15},{8,40},{9,1... | collective-permute-start | bytes 1966088 | tf_op jit(solution)/shard_map/ppermute | solution.py:42
  101.1 20.0 %collective-permute-start.32 = (bf16[160,2048]{1,0:T(8,128)(2,1)}, bf16[160,2048]{1,0:T(8,128)(2,1)S(1)}, u32[]{:S(2)}, u32[]{:S(2)}) collective-permute-start(bf16[160,2048]{1,0:T(8,128)(2,1)} %get-tuple-element.59), channel_id=1, source_target_pairs={{0,2},{1,3},{2,4},{3,5},{4,6},{5,7},{6,0},{7,1},{8,10},{9,11},{10,... | collective-permute-start | bytes 1966088 | tf_op jit(solution)/shard_map/ppermute | solution.py:42
  106.3 35.6 %collective-permute-start.12 = (bf16[5120,128]{1,0:T(8,128)(2,1)}, bf16[5120,128]{1,0:T(8,128)(2,1)}, u32[]{:S(2)}, u32[]{:S(2)}) collective-permute-start(bf16[5120,128]{1,0:T(8,128)(2,1)} %get-tuple-element.38.refs_0_), channel_id=1, source_target_pairs={{0,8},{1,33},{2,10},{3,35},{4,12},{5,37},{6,14},{7,39},{8,16},{9,4... | collective-permute-start | bytes 3932168 | tf_op jit(solution)/shard_map/ppermute | solution.py:42
  107.8 35.6 %collective-permute-start.14 = (bf16[5120,128]{1,0:T(8,128)(2,1)}, bf16[5120,128]{1,0:T(8,128)(2,1)}, u32[]{:S(2)}, u32[]{:S(2)}) collective-permute-start(bf16[5120,128]{1,0:T(8,128)(2,1)} %get-tuple-element.37.refs_1_), channel_id=1, source_target_pairs={{0,24},{1,97},{2,26},{3,99},{4,28},{5,101},{6,30},{7,103},{8,0},{9... | collective-permute-start | bytes 3932168 | tf_op jit(solution)/shard_map/ppermute | solution.py:42
  121.0 18.4 %collective-permute-start.36 = (bf16[160,2048]{1,0:T(8,128)(2,1)}, bf16[160,2048]{1,0:T(8,128)(2,1)S(1)}, u32[]{:S(2)}, u32[]{:S(2)}) collective-permute-start(bf16[160,2048]{1,0:T(8,128)(2,1)} %get-tuple-element.64), channel_id=1, source_target_pairs={{0,6},{1,7},{2,0},{3,1},{4,2},{5,3},{6,4},{7,5},{8,14},{9,15},{10,... | collective-permute-start | bytes 1966088 | tf_op jit(solution)/shard_map/ppermute | solution.py:42
  127.3 23.7 %collective-permute-start.34 = (bf16[160,2048]{1,0:T(8,128)(2,1)}, bf16[160,2048]{1,0:T(8,128)(2,1)S(1)}, u32[]{:S(2)}, u32[]{:S(2)}) collective-permute-start(bf16[160,2048]{1,0:T(8,128)(2,1)} %get-tuple-element.62), channel_id=1, source_target_pairs={{0,2},{1,3},{2,4},{3,5},{4,6},{5,7},{6,0},{7,1},{8,10},{9,11},{10,... | collective-permute-start | bytes 1966088 | tf_op jit(solution)/shard_map/ppermute | solution.py:42
  136.9 38.8 %collective-permute-start.10 = (bf16[5120,128]{1,0:T(8,128)(2,1)}, bf16[5120,128]{1,0:T(8,128)(2,1)}, u32[]{:S(2)}, u32[]{:S(2)}) collective-permute-start(bf16[5120,128]{1,0:T(8,128)(2,1)} %get-tuple-element.37.refs_1_), channel_id=1, source_target_pairs={{0,8},{1,33},{2,10},{3,35},{4,12},{5,37},{6,14},{7,39},{8,16},{9,4... | collective-permute-start | bytes 3932168 | tf_op jit(solution)/shard_map/ppermute | solution.py:42
  141.9 65.1 %collective-permute-start.11 = (bf16[5120,128]{1,0:T(8,128)(2,1)}, bf16[5120,128]{1,0:T(8,128)(2,1)}, u32[]{:S(2)}, u32[]{:S(2)}) collective-permute-start(bf16[5120,128]{1,0:T(8,128)(2,1)} %get-tuple-element.38.refs_0_), channel_id=1, source_target_pairs={{0,24},{1,97},{2,26},{3,99},{4,28},{5,101},{6,30},{7,103},{8,0},{9... | collective-permute-start | bytes 3932168 | tf_op jit(solution)/shard_map/ppermute | solution.py:42
  143.3 63.6 %collective-permute-start.13 = (bf16[5120,128]{1,0:T(8,128)(2,1)}, bf16[5120,128]{1,0:T(8,128)(2,1)}, u32[]{:S(2)}, u32[]{:S(2)}) collective-permute-start(bf16[5120,128]{1,0:T(8,128)(2,1)} %collective-permute-done.12.refs_0_), channel_id=1, source_target_pairs={{0,8},{1,33},{2,10},{3,35},{4,12},{5,37},{6,14},{7,39},{8,16},{9,4... | collective-permute-start | bytes 3932168 | tf_op jit(solution)/shard_map/ppermute | solution.py:42
  151.0 55.9 %collective-permute-start.15 = (bf16[5120,128]{1,0:T(8,128)(2,1)}, bf16[5120,128]{1,0:T(8,128)(2,1)}, u32[]{:S(2)}, u32[]{:S(2)}) collective-permute-start(bf16[5120,128]{1,0:T(8,128)(2,1)} %collective-permute-done.14.refs_1_), channel_id=1, source_target_pairs={{0,24},{1,97},{2,26},{3,99},{4,28},{5,101},{6,30},{7,103},{8,0},{9... | collective-permute-start | bytes 3932168 | tf_op jit(solution)/shard_map/ppermute | solution.py:42
  153.9 21.9 %collective-permute-start.19 = (bf16[128,2048]{1,0:T(8,128)(2,1)S(1)}, bf16[128,2048]{1,0:T(8,128)(2,1)}, u32[]{:S(2)}, u32[]{:S(2)}) collective-permute-start(bf16[128,2048]{1,0:T(8,128)(2,1)S(1)} %copy-done.17), channel_id=1, source_target_pairs={{0,2},{1,7},{2,4},{3,1},{4,6},{5,3},{6,0},{7,5},{8,10},{9,15},{10,... | collective-permute-start | bytes 1572872 | tf_op jit(solution)/shard_map/ppermute | solution.py:42
  161.6 120.0 %all-to-all-start.1 = ((bf16[16,24,2048]{2,1,0:T(8,128)(2,1)}), bf16[16,24,2048]{2,1,0:T(8,128)(2,1)S(1)}, u32[]{:S(2)}, u32[]{:S(2)}) async-start(bf16[16,24,2048]{2,1,0:T(8,128)(2,1)} %bitcast.13), calls=%async_computation.1 | async-start | bytes 3145728 | tf_op jit(solution)/shard_map/all_to_all | solution.py:319
  175.7 97.5 %collective-permute-start.20 = (bf16[128,2048]{1,0:T(8,128)(2,1)S(1)}, bf16[128,2048]{1,0:T(8,128)(2,1)S(1)}, u32[]{:S(2)}, u32[]{:S(2)}) collective-permute-start(bf16[128,2048]{1,0:T(8,128)(2,1)S(1)} %copy-done.17), channel_id=1, source_target_pairs={{0,6},{1,3},{2,0},{3,5},{4,2},{5,7},{6,4},{7,1},{8,14},{9,11},{10,... | collective-permute-start | bytes 1572872 | tf_op jit(solution)/shard_map/ppermute | solution.py:42
  175.7 97.5 %collective-permute-start.21 = (bf16[128,2048]{1,0:T(8,128)(2,1)}, bf16[128,2048]{1,0:T(8,128)(2,1)S(1)}, u32[]{:S(2)}, u32[]{:S(2)}) collective-permute-start(bf16[128,2048]{1,0:T(8,128)(2,1)} %collective-permute-done.19.refs_5_), channel_id=1, source_target_pairs={{0,2},{1,7},{2,4},{3,1},{4,6},{5,3},{6,0},{7,5},{8,10},{9,15},{10,... | collective-permute-start | bytes 1572872 | tf_op jit(solution)/shard_map/ppermute | solution.py:42
  256.9 18.8 %collective-permute-start.18 = (bf16[128,256]{1,0:T(8,128)(2,1)}, bf16[128,256]{1,0:T(8,128)(2,1)S(1)}, u32[]{:S(2)}, u32[]{:S(2)}) collective-permute-start(bf16[128,256]{1,0:T(8,128)(2,1)} %get-tuple-element.51), channel_id=1, source_target_pairs={{0,4},{1,5},{2,6},{3,7},{4,0},{5,1},{6,2},{7,3},{8,12},{9,13},{10,... | collective-permute-start | bytes 196616 | tf_op jit(solution)/shard_map/ppermute | solution.py:42
  (51 other events, 656.4 us)
